TPU v7x, 128 devices: a whole 4x4x4 slice. The times are simulated.
128 devices in a mesh: sp: 16 (over z, y), tp: 8 (over x, core).
Axes of the slice: x: 4, y: 4, z: 4, core: 2. Of those that a mesh axis runs over, the one named last changes fastest.
Arguments:
- queries: bfloat16 [16384, 1024], P('sp', 'tp'), may hold values from -8 to 8
- keyvals: bfloat16 [16384, 8, 128], P('sp', 'tp'), may hold values from -8 to 8
- head_sink_logit: float32 [16], P('tp'), may hold values from 2 to 7
- doc_ids: int32 [16384], P('sp'), may hold values from 0 to 7, never falling along the last dimension, each value on 1 to 4096 neighbouring positions
- stream_in: bfloat16 [16384, 2048], P(('sp', 'tp')), may hold values from -6 to 6
- out_weight: bfloat16 [1024, 2048], replicated, may hold values from -1.5 to 1.5
- first_gain: float32 [2048], replicated, may hold values from 0.1 to 1.9
- up_weight: bfloat16 [2048, 8192], P('sp', 'tp'), may hold values from -0.125 to 0.125
- down_weight: bfloat16 [8192, 2048], P('tp', 'sp'), may hold values from -0.0625 to 0.0625
- second_gain: float32 [2048], replicated, may hold values from 0.1 to 1.9
Outputs:
- layer_out: bfloat16 [16384, 2048], P(('sp', 'tp'))
Inputs may be any that keep to these rules, and one draw needn't show every extreme that they name: `doc_ids`: document numbers never fall along the sequence.
All inputs are finite; a program needn't handle non-finite values.
Results may differ from a plain program's by a relative error of at most 0.013.
Values may be sent and summed in bfloat16 or wider, within the bound.
A program may use at most 64 MiB of HBM per device.

v0:
```python
import jax
import jax.numpy as jnp
from jax import lax
from jax.sharding import Mesh
from jax.sharding import PartitionSpec as P

HEAD_SIZE = 64
WINDOW_REACH = 128
TP = ("tp_0", "tp_1")
SP_TP = ("sp", "tp_0", "tp_1")


NEG_LARGE = -1e30
NORM_EPS = 1e-05


def padded(block, sides, width):
    for axis, dim in sides:
        count = lax.axis_size(axis)
        forward = [(i, i + 1) for i in range(count - 1)]
        backward = [(target, source) for source, target in forward]
        low = lax.ppermute(
            lax.slice_in_dim(block, block.shape[dim] - width, None, axis=dim), axis, forward
        )
        high = lax.ppermute(lax.slice_in_dim(block, 0, width, axis=dim), axis, backward)
        block = jnp.concatenate([low, block, high], axis=dim)
    return block


def copy_for_each(x, axis):
    count = lax.axis_size(axis)
    return lax.all_to_all(jnp.broadcast_to(x[None], (count, *x.shape)), axis, 0, 0, tiled=True)


def joined_along(parts, dim):
    lengths = list(parts.shape[1:])
    lengths[dim] *= parts.shape[0]
    return jnp.moveaxis(parts, 0, dim).reshape(lengths)


def gather_axes(x, axes, dim):
    far, near = axes
    initial = copy_for_each(x, far)
    parts = jnp.swapaxes(copy_for_each(initial, near), 0, 1)
    return joined_along(parts.reshape(-1, *x.shape), dim)


def cut_along(x, dim, count):
    before, after = (x.shape[:dim], x.shape[dim + 1 :])
    return jnp.moveaxis(x.reshape(*before, count, -1, *after), dim, 0)


def summed_on_arrival(x, axis, dim):
    parts = cut_along(x, dim, lax.axis_size(axis))
    arrived = lax.all_to_all(parts, axis, split_axis=0, concat_axis=0, tiled=True)
    return arrived.astype(jnp.float32).sum(axis=0)


def sum_in_two_steps(x, axes, dim):
    far, near = axes
    own = summed_on_arrival(cut_along(x, dim, lax.axis_size(far)), near, dim + 1)
    return jnp.sum(
        lax.all_to_all(own.astype(jnp.bfloat16), far, 0, 0, tiled=True).astype(jnp.float32), axis=0
    )


def layer_norm(stream, gain_row):
    centre = jnp.mean(stream, axis=-1, keepdims=True)
    shifted = stream - centre
    spread = jnp.mean(shifted * shifted, axis=-1, keepdims=True)
    return shifted * lax.rsqrt(spread + NORM_EPS) * gain_row


def attend(queries, keyvals, head_sink_logit, doc_ids):
    tok_rows = queries.shape[0]
    kv_heads = keyvals.shape[1]
    heads_per_group = queries.shape[1] // (HEAD_SIZE * kv_heads)
    block_list = tok_rows // WINDOW_REACH
    score_scale = HEAD_SIZE ** (-0.5)
    doc_marks = doc_ids.astype(jnp.bfloat16)
    rim_keys, rim_docs = (
        padded(keyvals, (("sp", 0),), WINDOW_REACH),
        padded(doc_marks, (("sp", 0),), WINDOW_REACH),
    )
    padded_rows = rim_keys.reshape(block_list + 2, WINDOW_REACH, kv_heads, 2 * HEAD_SIZE)
    banded = jnp.concatenate([padded_rows[:-2], padded_rows[1:-1], padded_rows[2:]], axis=1)
    doc_ext = rim_docs.reshape(block_list + 2, WINDOW_REACH)
    doc_band = jnp.concatenate([doc_ext[:-2], doc_ext[1:-1], doc_ext[2:]], axis=1)
    offset = lax.axis_index("sp") * tok_rows
    total_rows = tok_rows * lax.axis_size("sp")
    query_pos = offset + jnp.arange(tok_rows, dtype=jnp.int32).reshape(block_list, WINDOW_REACH, 1)
    key_pos = (
        offset
        + (
            jnp.arange(block_list, dtype=jnp.int32)[:, None] * WINDOW_REACH
            + jnp.arange(3 * WINDOW_REACH, dtype=jnp.int32)[None, :]
            - WINDOW_REACH
        )[:, None, :]
    )
    allowed = (
        (jnp.abs(query_pos - key_pos) <= WINDOW_REACH)
        & (key_pos >= 0)
        & (key_pos < total_rows)
        & (doc_marks.reshape(block_list, WINDOW_REACH, 1) == doc_band[:, None, :])
    )
    query_block_list = queries.reshape(
        block_list, WINDOW_REACH, kv_heads, heads_per_group, HEAD_SIZE
    )
    scores = (
        jnp.einsum(
            "nqhgd,nkhd->nhgqk",
            query_block_list,
            banded[..., :HEAD_SIZE],
            preferred_element_type=jnp.float32,
        )
        * score_scale
    )
    scores = jnp.where(allowed[:, None, None], scores, NEG_LARGE)
    sink_col = head_sink_logit.reshape(kv_heads, heads_per_group)[None, :, :, None, None]
    highest = jnp.maximum(jnp.max(scores, axis=-1, keepdims=True), sink_col)
    powers = jnp.exp(scores - highest)
    denominator = jnp.sum(powers, axis=-1, keepdims=True) + jnp.exp(sink_col - highest)
    weights = (powers / denominator).astype(jnp.bfloat16)
    mixed_out = jnp.einsum(
        "nhgqk,nkhd->nqhgd", weights, banded[..., HEAD_SIZE:], preferred_element_type=jnp.float32
    )
    return mixed_out.astype(jnp.bfloat16).reshape(tok_rows, kv_heads * heads_per_group * HEAD_SIZE)


def per_device(
    queries,
    keyvals,
    head_sink_logit,
    doc_ids,
    stream_in,
    out_weight,
    first_gain,
    up_weight,
    down_weight,
    second_gain,
):
    up_whole = lax.all_gather(up_weight, "sp", axis=0, tiled=True)
    down_whole = lax.all_gather(down_weight, "sp", axis=1, tiled=True)
    attended = attend(queries, keyvals, head_sink_logit, doc_ids)
    tp_count = lax.axis_size(TP)
    own_rows = attended.shape[0] // tp_count
    by_peer = attended.reshape(tp_count, own_rows, attended.shape[1])
    projected = jnp.dot(
        lax.all_to_all(by_peer, TP, split_axis=0, concat_axis=2, tiled=True)[0],
        out_weight,
        preferred_element_type=jnp.float32,
    )[None][0]
    first_stream = layer_norm(stream_in.astype(jnp.float32) + projected, first_gain).astype(
        jnp.bfloat16
    )
    hidden = jnp.dot(
        gather_axes(first_stream, ("tp_0", "tp_1"), 0), up_whole, preferred_element_type=jnp.float32
    )
    active = jnp.square(jnp.maximum(hidden, 0.0)).astype(jnp.bfloat16)
    mixed_out = sum_in_two_steps(
        jnp.dot(active, down_whole, preferred_element_type=jnp.float32).astype(jnp.bfloat16),
        ("tp_0", "tp_1"),
        0,
    )
    return layer_norm(first_stream.astype(jnp.float32) + mixed_out, second_gain).astype(
        jnp.bfloat16
    )


def solution(mesh):
    finer = Mesh(mesh.devices.reshape(mesh.shape["sp"], 4, 2), ("sp", "tp_0", "tp_1"))
    placed = (
        P("sp", TP),
        P("sp", TP, None),
        P(TP),
        P("sp"),
        P(SP_TP, None),
        P(),
        P(),
        P("sp", TP),
        P(TP, "sp"),
        P(),
    )
    return jax.shard_map(
        per_device, mesh=finer, in_specs=placed, out_specs=P(SP_TP, None), check_vma=False
    )
```

profile of v0, /device:TPU:1, one launch (start us, length us, event | category | flops | bytes accessed | tf_op | source)
XLA Modules:
  0.0 190.7 jit_solution(34326995583364609)
XLA Ops:
  6.5 0.0 all-gather.3.cloned.1.call-start
  6.5 0.7 all-gather.3.cloned.1.call-update
  7.3 0.0 all-gather.5.cloned.1.call-start
  7.3 0.7 all-gather.5.cloned.1.call-update
  8.0 0.7 convert_element_type.39
  8.7 4.0 %collective-permute-start.2 = (bf16[128]{0:T(256)(128)(2,1)S(1)}, bf16[128]{0:T(256)(128)(2,1)S(1)}, u32[]{:S(2)}, u32[]{:S(2)}) collective-permute-start(bf16[128]{0:T(256)(128)(2,1)S(1)} %get-tuple-element.11), channel_id=1, source_target_pairs={{0,8},{8,16},{16,24},{24,32},{32,40},{40,48},{48,56},{56,64},{64,7... | collective-permute-start | bytes 776 | tf_op jit(solution)/shard_map/ppermute | solution.py:22
  12.7 1.3 collective-permute-start.3
  14.0 0.8 fusion.21
  14.8 4.0 %collective-permute-start = (bf16[128,1,128]{2,0,1:T(8,128)(2,1)S(1)}, bf16[128,1,128]{2,0,1:T(8,128)(2,1)S(1)}, u32[]{:S(2)}, u32[]{:S(2)}) collective-permute-start(bf16[128,1,128]{2,0,1:T(8,128)(2,1)S(1)} %get-tuple-element.7), channel_id=1, source_target_pairs={{0,8},{8,16},{16,24},{24,32},{32,40},{40,48},{48,56},{56,64},{64,7... | collective-permute-start | bytes 98312 | tf_op jit(solution)/shard_map/ppermute | solution.py:22
  18.8 1.3 collective-permute-start.1
  20.1 0.7 convert_bitcast_fusion
  20.8 0.1 fusion.15
  20.9 0.1 add_add_fusion
  21.0 1.1 copy.28
  22.1 1.2 reshape.201
  23.3 0.0 collective-permute-done.2
  23.3 0.0 collective-permute-done.3
  23.4 2.3 %fusion.6 = pred[8,128,384]{1,2,0:T(8,128)(4,1)S(1)} fusion(s32[8,384]{1,0:T(8,128)S(1)} %add_add_fusion, s32[8,128]{1,0:T(8,128)S(1)} %add_add_fusion.1, pred[8,384]{1,0:T(8,128)(4,1)S(1)} %get-tuple-element.14, pred[8,384]{1,0:T(8,128)(4,1)S(1)} %get-tuple-element.13, bf16[8,384]{1,0:T(8,128)(2,1)S(1)} %pad_maximum_fusion.3, ...), kind=kLoop, calls=%fused_computation.15 | loop fusion | flops 3538944 | bytes 423936 | tf_op jit(solution)/shard_map/and | solution.py:101
  25.7 0.0 collective-permute-done
  25.7 0.0 collective-permute-done.1
  25.7 1.1 pad_maximum_fusion.2
  26.8 0.2 copy.27
  27.0 0.2 copy.29
  27.2 0.0 copy-start.4
  27.2 0.1 pad_maximum_fusion
  27.3 0.7 fusion.1
  28.1 0.0 copy-done.4
  28.1 0.1 broadcast_maximum_fusion
  28.2 0.7 fusion
  28.9 0.1 exponential_add_fusion
  29.0 0.0 copy-start
  29.0 0.0 copy-start.1
  29.0 1.0 fusion.8
  30.0 12.2 %all_to_all.35 = bf16[8,128,128]{1,2,0:T(8,128)(2,1)S(1)} all-to-all(bf16[8,128,128]{1,2,0:T(8,128)(2,1)S(1)} %bitcast.72), channel_id=1, replica_groups=mesh['sp'=16,'tp_0'=4,'tp_1'=2] {'tp_0','tp_1'}, dimensions={0} | all-to-all | bytes 524288 | tf_op jit(solution)/shard_map/all_to_all | solution.py:149
  42.2 0.0 copy-done
  42.2 0.0 copy-done.1
  42.2 0.0 copy-start.2
  42.3 0.8 fusion.23
  43.1 0.3 multiply_reduce_fusion.1
  43.4 0.0 copy-done.2
  43.4 0.2 multiply_convert_fusion.2
  43.6 0.2 broadcast_in_dim.18
  43.8 27.9 %all_to_all.36 = bf16[4,128,2048]{2,1,0:T(8,128)(2,1)S(1)} all-to-all(bf16[4,128,2048]{2,1,0:T(8,128)(2,1)S(1)} %broadcast_in_dim.18), channel_id=1, replica_groups=mesh['sp'=16,'tp_0'=4,'tp_1'=2] {'tp_0'}, dimensions={0} | all-to-all | bytes 4194304 | tf_op jit(solution)/shard_map/all_to_all | solution.py:32
  71.7 0.5 broadcast_in_dim.19
  72.2 8.6 %all_to_all.37 = bf16[2,4,128,2048]{3,2,1,0:T(8,128)(2,1)S(1)} all-to-all(bf16[2,4,128,2048]{3,2,1,0:T(8,128)(2,1)S(1)} %broadcast_in_dim.19), channel_id=1, replica_groups=mesh['sp'=16,'tp_0'=4,'tp_1'=2] {'tp_1'}, dimensions={0} | all-to-all | bytes 8388608 | tf_op jit(solution)/shard_map/all_to_all | solution.py:32
  80.9 2.3 %copy.33 = bf16[2,4,128,2048]{3,2,0,1:T(8,128)(2,1)} copy(bf16[2,4,128,2048]{3,2,1,0:T(8,128)(2,1)S(1)} %all_to_all.37) | data formatting | bytes 8388608 | tf_op jit(solution)/shard_map/all_to_all | solution.py:32
  83.1 0.0 all-gather.3.cloned.1.call-done
  83.1 38.7 %all-gather.5.cloned.1.call-done = bf16[1024,2048]{1,0:T(8,128)(2,1)} async-done(((bf16[1024,128]{1,0:T(8,128)(2,1)}), bf16[1024,2048]{1,0:T(8,128)(2,1)}) %all-gather.5.cloned.1.call-update) | async-done | bytes 4194320 | tf_op jit(solution)/shard_map/all_gather | solution.py:143
  121.9 14.4 %convolution_convert_fusion = bf16[1024,2048]{1,0:T(8,128)(2,1)} fusion(bf16[1024,2048]{1,0:T(8,128)(2,1)} %all-gather.5.cloned.1.call-done, bf16[1024,2048]{1,0:T(8,128)(2,1)} %bitcast.66, bf16[2048,1024]{1,0:T(8,128)(2,1)} %all-gather.3.cloned.1.call-done), kind=kOutput, calls=%fused_computation.3 | convolution fusion | flops 8595177472 | bytes 16777216 | tf_op jit(solution)/shard_map/dot_general | solution.py:161
  136.3 2.5 %copy.45 = bf16[4,2,128,2048]{3,2,0,1:T(8,128)(2,1)S(1)} copy(bf16[4,2,128,2048]{3,2,1,0:T(8,128)(2,1)} %bitcast.67) | data formatting | bytes 8388608 | tf_op jit(solution)/shard_map/reshape;reshape | solution.py:50
  138.8 9.8 %all_to_all.38 = bf16[2,4,128,2048]{3,2,1,0:T(8,128)(2,1)} all-to-all(bf16[2,4,128,2048]{3,2,1,0:T(8,128)(2,1)S(1)} %bitcast.65), channel_id=1, replica_groups=mesh['sp'=16,'tp_0'=4,'tp_1'=2] {'tp_1'}, dimensions={0} | all-to-all | bytes 8388608 | tf_op jit(solution)/shard_map/all_to_all | solution.py:55
  148.6 3.5 %reduce_sum.69 = bf16[4,128,2048]{2,1,0:T(8,128)(2,1)S(1)} reduce(bf16[2,4,128,2048]{3,2,1,0:T(8,128)(2,1)} %all_to_all.38, bf16[]{:T(256)} %constant.37.clone.1), dimensions={0}, to_apply=%region_4.5 | reduce | flops 1048576 | bytes 6291458 | tf_op jit(solution)/shard_map/reduce_sum | solution.py:56
  152.1 29.2 %all_to_all.39 = bf16[4,128,2048]{2,1,0:T(8,128)(2,1)S(1)} all-to-all(bf16[4,128,2048]{2,1,0:T(8,128)(2,1)S(1)} %reduce_sum.69), channel_id=1, replica_groups=mesh['sp'=16,'tp_0'=4,'tp_1'=2] {'tp_0'}, dimensions={0} | all-to-all | bytes 4194304 | tf_op jit(solution)/shard_map/all_to_all | solution.py:63
  181.4 0.0 copy-start.3
  181.4 0.4 convert_reduce_fusion
  181.8 0.3 fusion.13
  182.1 0.4 multiply_reduce_fusion
  182.5 0.0 copy-done.3
  182.6 1.3 multiply_convert_fusion.1
  (9 shorter events, 0.1 us)
Async XLA Ops:
  6.5 76.6 %all-gather.3.cloned.1.call-start = ((), (), s32[]{:S(2)}) async-start(), calls=%async_computation.5 | async-start | bytes 4456448 | tf_op jit(solution)/shard_map/all_gather | solution.py:142
  7.3 114.6 %all-gather.5.cloned.1.call-start = ((), (), s32[]{:S(2)}) async-start(), calls=%async_computation.6 | async-start | bytes 4456448 | tf_op jit(solution)/shard_map/all_gather | solution.py:143
  8.7 14.6 %collective-permute-start.2 = (bf16[128]{0:T(256)(128)(2,1)S(1)}, bf16[128]{0:T(256)(128)(2,1)S(1)}, u32[]{:S(2)}, u32[]{:S(2)}) collective-permute-start(bf16[128]{0:T(256)(128)(2,1)S(1)} %get-tuple-element.11), channel_id=1, source_target_pairs={{0,8},{8,16},{16,24},{24,32},{32,40},{40,48},{48,56},{56,64},{64,7... | collective-permute-start | bytes 776 | tf_op jit(solution)/shard_map/ppermute | solution.py:22
  12.7 10.6 %collective-permute-start.3 = (bf16[128]{0:T(256)(128)(2,1)S(1)}, bf16[128]{0:T(256)(128)(2,1)S(1)}, u32[]{:S(2)}, u32[]{:S(2)}) collective-permute-start(bf16[128]{0:T(256)(128)(2,1)S(1)} %get-tuple-element.12), channel_id=1, source_target_pairs={{8,0},{16,8},{24,16},{32,24},{40,32},{48,40},{56,48},{64,56},{72,6... | collective-permute-start | bytes 776 | tf_op jit(solution)/shard_map/ppermute | solution.py:25
  14.8 10.9 %collective-permute-start = (bf16[128,1,128]{2,0,1:T(8,128)(2,1)S(1)}, bf16[128,1,128]{2,0,1:T(8,128)(2,1)S(1)}, u32[]{:S(2)}, u32[]{:S(2)}) collective-permute-start(bf16[128,1,128]{2,0,1:T(8,128)(2,1)S(1)} %get-tuple-element.7), channel_id=1, source_target_pairs={{0,8},{8,16},{16,24},{24,32},{32,40},{40,48},{48,56},{56,64},{64,7... | collective-permute-start | bytes 98312 | tf_op jit(solution)/shard_map/ppermute | solution.py:22
  18.8 6.9 %collective-permute-start.1 = (bf16[128,1,128]{2,0,1:T(8,128)(2,1)S(1)}, bf16[128,1,128]{2,0,1:T(8,128)(2,1)S(1)}, u32[]{:S(2)}, u32[]{:S(2)}) collective-permute-start(bf16[128,1,128]{2,0,1:T(8,128)(2,1)S(1)} %get-tuple-element.8), channel_id=1, source_target_pairs={{8,0},{16,8},{24,16},{32,24},{40,32},{48,40},{56,48},{64,56},{72,6... | collective-permute-start | bytes 98312 | tf_op jit(solution)/shard_map/ppermute | solution.py:25
  27.2 0.9 copy-start.4
  29.0 13.3 %copy-start = (bf16[1024,2048]{1,0:T(8,128)(2,1)S(1)}, bf16[1024,2048]{1,0:T(8,128)(2,1)}, u32[]{:S(2)}) copy-start(bf16[1024,2048]{1,0:T(8,128)(2,1)} %param.15) | copy-start | bytes 12582916
  29.0 13.2 %copy-start.1 = (bf16[128,2048]{1,0:T(8,128)(2,1)S(1)}, bf16[128,2048]{1,0:T(8,128)(2,1)}, u32[]{:S(2)}) copy-start(bf16[128,2048]{1,0:T(8,128)(2,1)} %param.14) | copy-start | bytes 1572868
  42.2 1.1 copy-start.2
  181.4 1.2 copy-start.3
Sparse Core Ops, SparseCore 0:
  9.5 54.8 all-gather.2
  66.5 55.3 all-gather.4
where the time goes:
time: 192 us; the launch traced here: 191 us
  blocking collectives  87.8 us (46%)
  waiting for transfers between devices  40.1 us (21%)
  matrix products  17 us (9%)
  between operations  13.6 us (7%)
  other arithmetic  12.4 us (6%)
  starting transfers between devices  10.6 us (6%)
  local copies, waits for them, and re-layouts  9.14 us (5%)
    all_gather x1, waiting for transfers between devices, per_device(): down_whole = lax.all_gather(down_weight, 'sp', axis=1, tiled=True)  38.7 us
    all_to_all x2, blocking collectives, copy_for_each(): lax.all_to_all(jnp.broadcast_to(x[None], (count, *x.shape)), axis, 0, 0,...  36.5 us
    all_to_all x1, blocking collectives, sum_in_two_steps(): lax.all_to_all(own.astype(jnp.bfloat16), far, 0, 0, tiled=True)  29.2 us
    dot_general x1, matrix products, per_device(): jnp.dot(active, down_whole, preferred_element_type=jnp.float32)  14.4 us
    all_to_all x1, blocking collectives, per_device(): lax.all_to_all(by_peer, TP, split_axis=0, concat_axis=2, tiled=True)[0]  12.2 us
    all_to_all x1, blocking collectives, summed_on_arrival(): lax.all_to_all(parts, axis, split_axis=0, concat_axis=0, tiled=True)  9.84 us
    ppermute x2, starting transfers between devices, padded(): lax.ppermute(lax.slice_in_dim(block, block.shape[dim] - width, None, axis...  7.98 us
  transfers between devices with their start and end apart: 6, of which 1 were waited for; matrix products, arithmetic and copies ran while one was open for 8% of the time, Pallas kernels for 0%

commit v1 on v0

v1 whole, which is shorter than its diff:
```python
import jax
import jax.numpy as jnp
from jax import lax
from jax.experimental import pallas as pl
from jax.experimental.pallas import tpu as pltpu
from jax.sharding import PartitionSpec as P

MESH = pl.DeviceIdType.MESH
F32 = jnp.float32
BF16 = jnp.bfloat16
NEG_LARGE = -1e30
NORM_EPS = 1e-05
R = 4
BLK = 128
D = 2048
HID = 1024
NCH = 8
CW = D // NCH

ORDER = [
    (0, 0), (1, 0), (3, 0), (0, 1), (0, 3), (3, 3), (3, 1), (1, 1),
    (1, 3), (2, 0), (0, 2), (3, 2), (2, 3), (2, 1), (1, 2), (2, 2),
]
RANK = {o: i for i, o in enumerate(ORDER)}


def nt_dot(a, b):
    return lax.dot_general(a, b, (((1,), (1,)), ((), ())), preferred_element_type=F32)


def dot(a, b):
    return jnp.dot(a, b, preferred_element_type=F32)


def normed(x, gain):
    centre = jnp.mean(x, axis=-1, keepdims=True)
    shifted = x - centre
    spread = jnp.mean(shifted * shifted, axis=-1, keepdims=True)
    return shifted * lax.rsqrt(spread + NORM_EPS) * gain


class Sems:
    def __init__(self):
        self.index = {}

    def at(self, key, count=1):
        if key not in self.index:
            self.index[key] = (sum(c for _, c in self.index.values()), count)
        return self.index[key][0]


def kernel(
    q_h, kv_h, sink_s, doc_h, st_h, ow_h, g1, up_h, dn_h, g2, out,
    qv, kvx, docv, doc_l, doc_r, docx, stv, owv, att_own, att_all, xbuf,
    up_all, dn_all, fs, act, psend, prx, pown, s1, s2, s3, mid_l, mid_r, fin_l, fin_r, macc,
    ss, rs, ls,
):
    sp, tp = lax.axis_index("sp"), lax.axis_index("tp")
    z, y = sp // R, sp % R
    x, core = tp // 2, tp % 2
    stride_a, stride_b = 1 + 3 * core, 4 - 3 * core
    a = y * (1 - core) + z * core
    b = z * (1 - core) + y * core

    def sp_of(da, db):
        return ((a + da) % R) * stride_a + ((b + db) % R) * stride_b

    partner = (sp, x * 2 + (1 - core))
    right = (sp, ((x + 1) % R) * 2 + core)
    left = (sp, ((x + R - 1) % R) * 2 + core)
    sp_next, sp_prev = (sp + 1) % 16, (sp + 15) % 16

    local_names = ["kv", "doc", "q", "up", "dn", "st", "ow"]
    own_up = up_all.at[pl.ds(pl.multiple_of(sp * BLK, BLK), BLK), :]
    pairs = {
        "kv": (kv_h, kvx.at[pl.ds(BLK, 1024), :]),
        "doc": (doc_h, docv),
        "q": (q_h, qv),
        "up": (up_h, own_up),
        "dn": (dn_h, dn_all.at[:, pl.ds(0, BLK)]),
        "st": (st_h, stv),
        "ow": (ow_h, owv),
    }
    local = {n: pltpu.make_async_copy(*pairs[n], ls.at[i]) for i, n in enumerate(local_names)}
    for n in local_names:
        local[n].start()

    barrier = pltpu.get_barrier_semaphore()
    greet = [(sp, (tp + i) % 8) for i in range(1, 8)]
    greet += [(sp_of(da, db), tp) for da, db in ((1, 0), (3, 0), (0, 1), (0, 3))]
    greet += [(sp_next, tp), (sp_prev, tp)]
    for dev in greet:
        pl.semaphore_signal(barrier, inc=1, device_id=dev, device_id_type=MESH)
    pl.semaphore_wait(barrier, len(greet))

    sems = Sems()
    sent = []
    waited = set()
    arriving = {}

    def send(key, src, dst, dev):
        i = sems.at(key)
        copy = pltpu.make_async_remote_copy(
            src_ref=src, dst_ref=dst, send_sem=ss.at[i], recv_sem=rs.at[i], device_id=dev, device_id_type=MESH
        )
        copy.start()
        sent.append(copy)
        arriving[key] = copy

    def arrive(key):
        if key not in waited:
            waited.add(key)
            arriving[key].wait_recv()

    local["kv"].wait()
    local["doc"].wait()
    send("kv_l", kvx.at[pl.ds(1024, BLK), :], kvx.at[pl.ds(0, BLK), :], (sp_next, tp))
    send("kv_r", kvx.at[pl.ds(BLK, BLK), :], kvx.at[pl.ds(1024 + BLK, BLK), :], (sp_prev, tp))
    send("doc_l", docv, doc_l, (sp_next, tp))
    send("doc_r", docv, doc_r, (sp_prev, tp))

    def block(w, origin, at, half):
        da, db = origin
        if w == "u":
            lo, n = {None: (0, BLK), 0: (0, BLK // 2), 1: (BLK // 2, BLK // 2)}[half]
            return up_all.at[pl.ds(pl.multiple_of(sp_of(da, db) * BLK + lo, BLK // 2), n), :]
        lo, n = {None: (0, HID), 0: (0, HID // 2), 1: (HID // 2, HID // 2)}[half]
        ra, rb = (da - at[0]) % R, (db - at[1]) % R
        r0, r1 = RANK[(ra, rb)], RANK[(rb, ra)]
        slot = r0 + core * (r1 - r0)
        return dn_all.at[pl.ds(lo, n), pl.ds(pl.multiple_of(slot * BLK, BLK), BLK)]

    def pass_on(w, origin, to, half=None):
        rel = ((origin[0] - to[0]) % R, (origin[1] - to[1]) % R)
        send(
            (w, rel, half), block(w, origin, (0, 0), half), block(w, origin, to, half),
            (sp_of(to[0] % R, to[1] % R), tp),
        )

    AP, AM, BP, BM = (1, 0), (-1, 0), (0, 1), (0, -1)
    relayed = set()

    def need(w, origin):
        if (w, origin) in relayed:
            return
        relayed.add((w, origin))
        if origin == (2, 0):
            arrive((w, origin, 0))
            arrive((w, origin, 1))
        else:
            arrive((w, origin, None))
        if origin == (3, 0):
            pass_on(w, origin, AP, 0)
        if origin == (1, 0):
            pass_on(w, origin, AM, 1)
        if origin in ((3, 0), (1, 0), (2, 0)):
            pass_on(w, origin, BP)
            pass_on(w, origin, BM)
        if origin in ((0, 3), (2, 3)):
            pass_on(w, origin, BP)
        if origin in ((3, 1), (1, 1)):
            pass_on(w, origin, BM)

    local["up"].wait()
    for to in (AP, AM, BP, BM):
        pass_on("u", (0, 0), to)
    local["dn"].wait()
    for to in (AP, AM):
        pass_on("d", (0, 0), to)

    local["q"].wait()
    docx[pl.ds(8, 8), :] = docv[...].astype(F32)
    row = lax.broadcasted_iota(jnp.int32, (BLK, BLK), 0)
    col = lax.broadcasted_iota(jnp.int32, (BLK, BLK), 1)
    low = col < 64
    a2a = sems.at("a2a", 8)

    def attend(blk):
        rows = pl.ds(pl.multiple_of(blk * BLK, BLK), BLK)
        qf = qv[rows, :].astype(F32) * 0.125
        q2 = jnp.concatenate(
            [jnp.where(low, qf, 0.0), jnp.where(low, pltpu.roll(qf, 64, 1), 0.0)], axis=0
        ).astype(BF16)
        kvb = kvx[pl.ds(pl.multiple_of(blk * BLK, BLK), 3 * BLK), :]
        s = nt_dot(q2, kvb)
        dq = jnp.broadcast_to(docx[pl.ds(blk + 8, 1), :], (BLK, BLK)).T
        same = [jnp.broadcast_to(docx[pl.ds(blk + 7 + j, 1), :], (BLK, BLK)) == dq for j in range(3)]
        same[0] = same[0] & (col >= row)
        same[2] = same[2] & (col <= row)
        weights, scale = [], []
        for h in range(2):
            sink = sink_s[h]
            t = [
                jnp.where(same[j], s[h * BLK : (h + 1) * BLK, j * BLK : (j + 1) * BLK], NEG_LARGE)
                for j in range(3)
            ]
            top = jnp.max(jnp.maximum(jnp.maximum(t[0], t[1]), t[2]), axis=-1, keepdims=True)
            top = jnp.maximum(top, sink)
            p = [jnp.exp(v - top) for v in t]
            total = jnp.sum(p[0] + p[1] + p[2], axis=-1, keepdims=True) + jnp.exp(sink - top)
            weights.append(jnp.concatenate(p, axis=1).astype(BF16))
            scale.append(1.0 / total)
        o = dot(jnp.concatenate(weights, axis=0), kvb)
        o0, o1 = o[:BLK] * scale[0], o[BLK:] * scale[1]
        att_own[rows, :] = jnp.where(low, pltpu.roll(o0, 64, 1), o1).astype(BF16)
        mine = pl.ds(pl.multiple_of(tp * BLK, BLK), BLK)

        @pl.when(blk != tp)
        def _():
            pltpu.make_async_remote_copy(
                src_ref=att_own.at[rows, :], dst_ref=att_all.at[:, mine],
                send_sem=ss.at[a2a + blk], recv_sem=rs.at[a2a + tp],
                device_id=(sp, blk), device_id_type=MESH,
            ).start()

        @pl.when(blk == tp)
        def _():
            att_all[:, mine] = att_own[rows, :]

    def inner(i, carry):
        attend(i)
        return carry

    lax.fori_loop(1, 7, inner, 0)
    for key in ("kv_l", "kv_r", "doc_l", "doc_r"):
        arrive(key)
    docx[pl.ds(0, 8), :] = jnp.where(sp == 0, -1.0, doc_l[...].astype(F32))
    docx[pl.ds(16, 8), :] = jnp.where(sp == 15, -1.0, doc_r[...].astype(F32))

    def outer(i, carry):
        attend(i * 7)
        return carry

    lax.fori_loop(0, 2, outer, 0)

    def a2a_copy(i):
        other = (tp + i) % 8
        return pltpu.make_async_remote_copy(
            src_ref=att_own.at[pl.ds(pl.multiple_of(other * BLK, BLK), BLK), :],
            dst_ref=att_all.at[:, pl.ds(pl.multiple_of(other * BLK, BLK), BLK)],
            send_sem=ss.at[a2a + other], recv_sem=rs.at[a2a + other],
            device_id=(sp, other), device_id_type=MESH,
        )

    local["ow"].wait()
    local["st"].wait()
    for i in range(1, 8):
        a2a_copy(i).wait_recv()

    def project(n, carry):
        cols = pl.ds(pl.multiple_of(n * 256, 256), 256)
        xbuf[:, cols] = dot(att_all[...], owv[:, cols]) + stv[:, cols].astype(F32)
        return carry

    lax.fori_loop(0, 8, project, 0)
    need("u", (3, 0))
    need("u", (1, 0))
    need("u", (0, 3))

    HALF = BLK // 2
    half = lambda h: pl.ds(h * HALF, HALF)

    def fs_send(name, src, dst, h, dev):
        send((name, h), fs.at[src[0], src[1], half(h), :], fs.at[dst[0], dst[1], half(h), :], dev)

    for h in range(2):
        fs[0, 0, half(h), :] = normed(xbuf[half(h), :], g1[...]).astype(BF16)
        if h == 0:
            fs_send("x_l", (0, 0), (0, 3), 0, right)
    fs_send("x_r", (0, 0), (0, 1), 1, left)
    fs_send("x_l", (0, 0), (0, 3), 1, right)
    fs_send("x_r", (0, 0), (0, 1), 0, left)
    for h in range(2):
        fs_send("c0", (0, 0), (1, 0), h, partner)

    def gather_rows(name, h):
        arrive((name, h))
        if name == "x_l":
            if h == 0:
                fs_send("x_2", (0, 3), (0, 2), 0, right)
            fs_send("c3", (0, 3), (1, 3), h, partner)
        elif name == "x_r":
            if h == 1:
                fs_send("x_2", (0, 1), (0, 2), 1, left)
            fs_send("c1", (0, 1), (1, 1), h, partner)
        elif name == "x_2":
            fs_send("c2", (0, 2), (1, 2), h, partner)

    def hidden(dx):
        for h in range(2):
            arrive((f"c{dx}", h))

        def part(n, carry):
            cols = pl.ds(pl.multiple_of(n * 256, 256), 256)
            rows = fs[:, dx].reshape(2 * BLK, D)
            v = jnp.maximum(dot(rows, up_all[:, cols]), 0.0)
            act[:, dx, :, cols] = (v * v).astype(BF16).reshape(2, BLK, 256)
            return carry

        lax.fori_loop(0, HID // 256, part, 0)

    need("u", (2, 0))
    for to in (BP, BM):
        pass_on("d", (0, 0), to)
    need("d", (3, 0))
    need("d", (1, 0))
    need("u", (3, 1))
    gather_rows("x_l", 0)
    gather_rows("x_r", 1)
    need("u", (1, 1))
    need("d", (0, 3))
    need("u", (2, 3))
    need("d", (2, 0))
    gather_rows("x_l", 1)
    gather_rows("x_r", 0)
    for da in range(R):
        for db in range(R):
            if (da, db) != (0, 0):
                need("u", (da, db))
    hidden(0)
    hidden(1)
    need("d", (3, 1))
    hidden(3)
    gather_rows("x_2", 0)
    gather_rows("x_2", 1)
    hidden(2)

    def cols_of(rank):
        dy, dz = ORDER[rank]
        return pl.ds(pl.multiple_of((((z + dz) % R) * R + (y + dy) % R) * BLK, BLK), BLK)

    def product(j):
        for o in (ORDER[2 * j], ORDER[2 * j + 1]):
            for origin in (o, (o[1], o[0])):
                if origin != (0, 0):
                    need("d", origin)
        cols = pl.ds(j * CW, CW)
        psend[j] = dot(act[1].reshape(4 * BLK, HID), dn_all[:, cols]).astype(BF16).reshape(R, BLK, CW)
        send(("p", j), psend.at[j], prx.at[j], partner)
        pown[j] = dot(act[0].reshape(4 * BLK, HID), dn_all[:, cols]).reshape(R, BLK, CW)

    def pair_sum(j):
        arrive(("p", j))
        s2[j] = (pown[j, 2] + prx[j, 2].astype(F32)).astype(BF16)
        send(("mid_l", j), s2.at[j, pl.ds(0, HALF), :], mid_l.at[j], right)
        send(("mid_r", j), s2.at[j, pl.ds(HALF, HALF), :], mid_r.at[j], left)
        mine = pown[j, 0] + prx[j, 0].astype(F32)
        for i in range(2):
            macc[:, cols_of(2 * j + i)] = mine[:, i * BLK : (i + 1) * BLK]

    def middle(j):
        lo, hi = pl.ds(0, HALF), pl.ds(HALF, HALF)
        s1[j, hi, :] = (pown[j, 1, hi, :] + prx[j, 1, hi, :].astype(F32)).astype(BF16)
        s3[j, lo, :] = (pown[j, 3, lo, :] + prx[j, 3, lo, :].astype(F32)).astype(BF16)
        arrive(("mid_l", j))
        s1[j, lo, :] = (pown[j, 1, lo, :] + prx[j, 1, lo, :].astype(F32) + mid_l[j].astype(F32)).astype(BF16)
        send(("fin_l", j), s1.at[j], fin_l.at[j], right)
        arrive(("mid_r", j))
        s3[j, hi, :] = (pown[j, 3, hi, :] + prx[j, 3, hi, :].astype(F32) + mid_r[j].astype(F32)).astype(BF16)
        send(("fin_r", j), s3.at[j], fin_r.at[j], left)

    def total_sum(j):
        arrive(("fin_l", j))
        arrive(("fin_r", j))
        v = fin_l[j].astype(F32) + fin_r[j].astype(F32)
        for i in range(2):
            macc[:, cols_of(2 * j + i)] += v[:, i * BLK : (i + 1) * BLK]

    for i in range(NCH + 6):
        if i < NCH:
            product(i)
        if 0 <= i - 1 < NCH:
            pair_sum(i - 1)
        if 0 <= i - 3 < NCH:
            middle(i - 3)
        if 0 <= i - 6 < NCH:
            total_sum(i - 6)

    for h in range(2):
        v = fs[0, 0, half(h), :].astype(F32) + macc[half(h), :]
        out[half(h), :] = normed(v, g2[...]).astype(BF16)

    for copy in sent:
        copy.wait_send()
    for i in range(1, 8):
        a2a_copy(i).wait_send()


def per_device(q, kv, sink, doc, stream, ow, g1, up, dn, g2):
    vm, anyw = pl.BlockSpec(memory_space=pltpu.VMEM), pl.BlockSpec(memory_space=pl.ANY)
    smem = pl.BlockSpec(memory_space=pltpu.SMEM)
    return pl.pallas_call(
        kernel,
        out_shape=jax.ShapeDtypeStruct(stream.shape, BF16),
        in_specs=[anyw, anyw, smem, anyw, anyw, anyw, vm, anyw, anyw, vm],
        out_specs=vm,
        scratch_shapes=[
            pltpu.VMEM((1024, BLK), BF16),
            pltpu.VMEM((1024 + 2 * BLK, BLK), BF16),
            pltpu.VMEM((8, BLK), jnp.int32),
            pltpu.VMEM((8, BLK), jnp.int32),
            pltpu.VMEM((8, BLK), jnp.int32),
            pltpu.VMEM((24, BLK), F32),
            pltpu.VMEM((BLK, D), BF16),
            pltpu.VMEM((1024, D), BF16),
            pltpu.VMEM((1024, BLK), BF16),
            pltpu.VMEM((BLK, 1024), BF16),
            pltpu.VMEM((BLK, D), F32),
            pltpu.VMEM((D, HID), BF16),
            pltpu.VMEM((HID, D), BF16),
            pltpu.VMEM((2, R, BLK, D), BF16),
            pltpu.VMEM((2, R, BLK, HID), BF16),
            pltpu.VMEM((NCH, R, BLK, CW), BF16),
            pltpu.VMEM((NCH, R, BLK, CW), BF16),
            pltpu.VMEM((NCH, R, BLK, CW), F32),
            pltpu.VMEM((NCH, BLK, CW), BF16),
            pltpu.VMEM((NCH, BLK, CW), BF16),
            pltpu.VMEM((NCH, BLK, CW), BF16),
            pltpu.VMEM((NCH, BLK // 2, CW), BF16),
            pltpu.VMEM((NCH, BLK // 2, CW), BF16),
            pltpu.VMEM((NCH, BLK, CW), BF16),
            pltpu.VMEM((NCH, BLK, CW), BF16),
            pltpu.VMEM((BLK, D), F32),
            pltpu.SemaphoreType.DMA((112,)),
            pltpu.SemaphoreType.DMA((112,)),
            pltpu.SemaphoreType.DMA((8,)),
        ],
        compiler_params=pltpu.CompilerParams(
            collective_id=0, has_side_effects=True, vmem_limit_bytes=60 * 1024 * 1024
        ),
        name="layer",
    )(
        q, kv.reshape(1024, BLK), sink, doc.reshape(8, BLK), stream, ow, g1.reshape(1, D), up, dn, g2.reshape(1, D)
    )


def solution(mesh):
    placed = (
        P("sp", "tp"),
        P("sp", "tp", None),
        P("tp"),
        P("sp"),
        P(("sp", "tp"), None),
        P(),
        P(),
        P("sp", "tp"),
        P("tp", "sp"),
        P(),
    )
    return jax.shard_map(
        per_device, mesh=mesh, in_specs=placed, out_specs=P(("sp", "tp"), None), check_vma=False
    )
```

time: 192 us -> 86.6 us (0.45)
  blocking collectives: 87.8 us -> 0 us
  Pallas kernels: 0 us -> 84.5 us
  waiting for transfers between devices: 40.1 us -> 0 us
  matrix products: 17 us -> 0 us
  between operations: 13.6 us -> 0.01 us
  other arithmetic: 12.4 us -> 0 us
  starting transfers between devices: 10.6 us -> 0 us
  local copies, waits for them, and re-layouts: 9.14 us -> 1.88 us
    all_to_all x5 -> x0, blocking collectives: 87.8 us -> none  [the longest x2 36.5 us: copy_for_each(): lax.all_to_all(jnp.broadcast_to(x[None], (count, *x.shape)), axis, 0, 0,...]
    pallas_call x0 -> x1, Pallas kernels: none -> 84.5 us  [per_device(): pl.pallas_call(kernel, out_shape=jax.ShapeDtypeStruct(stream.shape, BF16)...]
    all_gather x2 -> x0, waiting for transfers between devices: 38.7 us -> none  [the longest x1 38.7 us: per_device(): down_whole = lax.all_gather(down_weight, 'sp', axis=1, tiled=True)]
    dot_general x4 -> x0, matrix products: 17 us -> none  [the longest x1 14.4 us: per_device(): jnp.dot(active, down_whole, preferred_element_type=jnp.float32)]
    ppermute x4 -> x0, starting transfers between devices: 10.6 us -> none  [the longest x2 7.98 us: padded(): lax.ppermute(lax.slice_in_dim(block, block.shape[dim] - width, None, axis...]
    reduce_sum x6 -> x0, other arithmetic: 5.68 us -> none  [the longest x1 3.55 us: summed_on_arrival(): return arrived.astype(jnp.float32).sum(axis=0)]
    another operation x2 -> x0, local copies, waits for them, and re-layouts: 3.71 us -> none  [the longest x1 2.49 us: cut_along(): return jnp.moveaxis(x.reshape(*before, count, -1, *after), dim, 0)]
    slice x5 -> x0, local copies, waits for them, and re-layouts: 2.33 us -> none  [the longest x1 1.14 us: attend(): padded_rows[1:-1]]
  transfers between devices with their start and end apart: 6 -> 0, of which waited for: 1 -> 0; matrix products, arithmetic and copies ran while one was open for 8% -> 0% of each run, Pallas kernels for 0% -> 0%
where the time goes in v1:
time: 86.6 us; the launch traced here: 86.4 us
  Pallas kernels  84.5 us (98%)
  local copies, waits for them, and re-layouts  1.88 us (2%)
    pallas_call x1, Pallas kernels, per_device(): pl.pallas_call(kernel, out_shape=jax.ShapeDtypeStruct(stream.shape, BF16)...  84.5 us
    unnamed x1, local copies, waits for them, and re-layouts  1.88 us

profile of v1, /device:TPU:1, one launch (start us, length us, event | category | flops | bytes accessed | tf_op | source)
XLA Modules:
  0.0 86.4 jit_solution(4219365655152828724)
XLA Ops:
  0.0 84.5 %layer.1 = bf16[128,2048]{1,0:T(8,128)(2,1)} custom-call(bf16[1024,128]{1,0:T(8,128)(2,1)} %q_h.1, bf16[1024,128]{1,0:T(8,128)(2,1)} %bitcast.4, f32[2]{0:T(128)} %sink_s.1, s32[8,128]{1,0:T(8,128)} %bitcast.7, bf16[128,2048]{1,0:T(8,128)(2,1)} %st_h.1, bf16[1024,2048]{1,0:T(8,128)(2,1)} %ow_h.1, f32[1,2048]{1,0:T(1,128)} %bitcast.5, ...), custom_call_target="tpu_custom_call" | custom-call | tf_op jit(solution)/shard_map/layer/pallas_call | solution.py:392
  84.5 1.9 %copy.12 = bf16[128,2048]{1,0:T(8,128)(2,1)} copy(bf16[128,2048]{1,0:T(8,128)(2,1)} %layer.1) | data formatting | bytes 1048576

commit v2 on v1

--- a/solution.py
+++ b/solution.py
@@ -1,3 +1,5 @@
+import functools
+
 import jax
 import jax.numpy as jnp
 from jax import lax
@@ -37,6 +39,19 @@
     shifted = x - centre
     spread = jnp.mean(shifted * shifted, axis=-1, keepdims=True)
     return shifted * lax.rsqrt(spread + NORM_EPS) * gain
+
+
+def scoped(name):
+    def wrap(f):
+        @functools.wraps(f)
+        def run(*args):
+            tag = "_".join("".join(c for c in str(v) if c.isalnum()) for v in args if isinstance(v, (int, str, tuple)))
+            with jax.named_scope(f"{name}#v={tag}"):
+                return f(*args)
+
+        return run
+
+    return wrap
 
 
 class Sems:
@@ -140,6 +155,7 @@
     AP, AM, BP, BM = (1, 0), (-1, 0), (0, 1), (0, -1)
     relayed = set()
 
+    @scoped("need")
     def need(w, origin):
         if (w, origin) in relayed:
             return
@@ -160,13 +176,17 @@
             pass_on(w, origin, BP)
         if origin in ((3, 1), (1, 1)):
             pass_on(w, origin, BM)
+        if (w, origin) == ("u", (1, 1)):
+            local["dn"].wait()
+            pass_on("d", (0, 0), BP)
+            pass_on("d", (0, 0), BM)
+        if (w, origin) == ("u", (2, 3)):
+            pass_on("d", (0, 0), AP)
+            pass_on("d", (0, 0), AM)
 
     local["up"].wait()
-    for to in (AP, AM, BP, BM):
+    for to in (AP, AM):
         pass_on("u", (0, 0), to)
-    local["dn"].wait()
-    for to in (AP, AM):
-        pass_on("d", (0, 0), to)
 
     local["q"].wait()
     docx[pl.ds(8, 8), :] = docv[...].astype(F32)
@@ -175,7 +195,7 @@
     low = col < 64
     a2a = sems.at("a2a", 8)
 
-    def attend(blk):
+    def attended(blk):
         rows = pl.ds(pl.multiple_of(blk * BLK, BLK), BLK)
         qf = qv[rows, :].astype(F32) * 0.125
         q2 = jnp.concatenate(
@@ -202,7 +222,10 @@
             scale.append(1.0 / total)
         o = dot(jnp.concatenate(weights, axis=0), kvb)
         o0, o1 = o[:BLK] * scale[0], o[BLK:] * scale[1]
-        att_own[rows, :] = jnp.where(low, pltpu.roll(o0, 64, 1), o1).astype(BF16)
+        return jnp.where(low, pltpu.roll(o0, 64, 1), o1).astype(BF16)
+
+    def hand_out(blk):
+        rows = pl.ds(pl.multiple_of(blk * BLK, BLK), BLK)
         mine = pl.ds(pl.multiple_of(tp * BLK, BLK), BLK)
 
         @pl.when(blk != tp)
@@ -217,21 +240,34 @@
         def _():
             att_all[:, mine] = att_own[rows, :]
 
+    @scoped("attend")
+    def attend(first, second):
+        values = [attended(first), attended(second)]
+        for blk, v in zip((first, second), values):
+            att_own[pl.ds(pl.multiple_of(blk * BLK, BLK), BLK), :] = v
+        for blk in (first, second):
+            hand_out(blk)
+
     def inner(i, carry):
-        attend(i)
+        attend(2 * i + 1, 2 * i + 2)
         return carry
 
-    lax.fori_loop(1, 7, inner, 0)
+    lax.fori_loop(0, 2, inner, 0)
+    for to in (BP, BM):
+        pass_on("u", (0, 0), to)
+    lax.fori_loop(2, 3, inner, 0)
     for key in ("kv_l", "kv_r", "doc_l", "doc_r"):
         arrive(key)
     docx[pl.ds(0, 8), :] = jnp.where(sp == 0, -1.0, doc_l[...].astype(F32))
     docx[pl.ds(16, 8), :] = jnp.where(sp == 15, -1.0, doc_r[...].astype(F32))
 
     def outer(i, carry):
-        attend(i * 7)
+        attend(i, i + 7)
         return carry
 
-    lax.fori_loop(0, 2, outer, 0)
+    lax.fori_loop(0, 1, outer, 0)
+    need("u", (3, 0))
+    need("u", (1, 0))
 
     def a2a_copy(i):
         other = (tp + i) % 8
@@ -242,19 +278,25 @@
             device_id=(sp, other), device_id_type=MESH,
         )
 
-    local["ow"].wait()
-    local["st"].wait()
-    for i in range(1, 8):
-        a2a_copy(i).wait_recv()
-
-    def project(n, carry):
-        cols = pl.ds(pl.multiple_of(n * 256, 256), 256)
+    @scoped("a2a_wait")
+    def a2a_wait():
+        local["ow"].wait()
+        local["st"].wait()
+        for i in range(1, 8):
+            a2a_copy(i).wait_recv()
+
+    a2a_wait()
+
+    def project(n):
+        cols = pl.ds(n * 512, 512)
         xbuf[:, cols] = dot(att_all[...], owv[:, cols]) + stv[:, cols].astype(F32)
-        return carry
-
-    lax.fori_loop(0, 8, project, 0)
-    need("u", (3, 0))
-    need("u", (1, 0))
+
+    @scoped("projection")
+    def projection():
+        for n in range(4):
+            project(n)
+
+    projection()
     need("u", (0, 3))
 
     HALF = BLK // 2
@@ -263,8 +305,12 @@
     def fs_send(name, src, dst, h, dev):
         send((name, h), fs.at[src[0], src[1], half(h), :], fs.at[dst[0], dst[1], half(h), :], dev)
 
+    @scoped("first_norm")
+    def first_norm(h):
+        fs[0, 0, half(h), :] = normed(xbuf[half(h), :], g1[...]).astype(BF16)
+
     for h in range(2):
-        fs[0, 0, half(h), :] = normed(xbuf[half(h), :], g1[...]).astype(BF16)
+        first_norm(h)
         if h == 0:
             fs_send("x_l", (0, 0), (0, 3), 0, right)
     fs_send("x_r", (0, 0), (0, 1), 1, left)
@@ -273,6 +319,7 @@
     for h in range(2):
         fs_send("c0", (0, 0), (1, 0), h, partner)
 
+    @scoped("gather_rows")
     def gather_rows(name, h):
         arrive((name, h))
         if name == "x_l":
@@ -286,49 +333,46 @@
         elif name == "x_2":
             fs_send("c2", (0, 2), (1, 2), h, partner)
 
+    @scoped("hidden")
     def hidden(dx):
         for h in range(2):
             arrive((f"c{dx}", h))
 
-        def part(n, carry):
-            cols = pl.ds(pl.multiple_of(n * 256, 256), 256)
+        for n in range(HID // 256):
+            cols = pl.ds(n * 256, 256)
             rows = fs[:, dx].reshape(2 * BLK, D)
             v = jnp.maximum(dot(rows, up_all[:, cols]), 0.0)
             act[:, dx, :, cols] = (v * v).astype(BF16).reshape(2, BLK, 256)
-            return carry
-
-        lax.fori_loop(0, HID // 256, part, 0)
 
     need("u", (2, 0))
-    for to in (BP, BM):
-        pass_on("d", (0, 0), to)
+    need("u", (3, 1))
+    need("u", (1, 1))
+    gather_rows("x_l", 0)
+    gather_rows("x_r", 1)
+    need("u", (2, 3))
+    gather_rows("x_l", 1)
+    gather_rows("x_r", 0)
+    need("d", (0, 3))
     need("d", (3, 0))
     need("d", (1, 0))
-    need("u", (3, 1))
-    gather_rows("x_l", 0)
-    gather_rows("x_r", 1)
-    need("u", (1, 1))
-    need("d", (0, 3))
-    need("u", (2, 3))
-    need("d", (2, 0))
-    gather_rows("x_l", 1)
-    gather_rows("x_r", 0)
+    gather_rows("x_2", 0)
+    gather_rows("x_2", 1)
     for da in range(R):
         for db in range(R):
             if (da, db) != (0, 0):
                 need("u", (da, db))
     hidden(0)
     hidden(1)
+    need("d", (2, 0))
+    hidden(3)
     need("d", (3, 1))
-    hidden(3)
-    gather_rows("x_2", 0)
-    gather_rows("x_2", 1)
     hidden(2)
 
     def cols_of(rank):
         dy, dz = ORDER[rank]
         return pl.ds(pl.multiple_of((((z + dz) % R) * R + (y + dy) % R) * BLK, BLK), BLK)
 
+    @scoped("product")
     def product(j):
         for o in (ORDER[2 * j], ORDER[2 * j + 1]):
             for origin in (o, (o[1], o[0])):
@@ -339,6 +383,7 @@
         send(("p", j), psend.at[j], prx.at[j], partner)
         pown[j] = dot(act[0].reshape(4 * BLK, HID), dn_all[:, cols]).reshape(R, BLK, CW)
 
+    @scoped("pair_sum")
     def pair_sum(j):
         arrive(("p", j))
         s2[j] = (pown[j, 2] + prx[j, 2].astype(F32)).astype(BF16)
@@ -348,6 +393,7 @@
         for i in range(2):
             macc[:, cols_of(2 * j + i)] = mine[:, i * BLK : (i + 1) * BLK]
 
+    @scoped("middle")
     def middle(j):
         lo, hi = pl.ds(0, HALF), pl.ds(HALF, HALF)
         s1[j, hi, :] = (pown[j, 1, hi, :] + prx[j, 1, hi, :].astype(F32)).astype(BF16)
@@ -359,6 +405,7 @@
         s3[j, hi, :] = (pown[j, 3, hi, :] + prx[j, 3, hi, :].astype(F32) + mid_r[j].astype(F32)).astype(BF16)
         send(("fin_r", j), s3.at[j], fin_r.at[j], left)
 
+    @scoped("total_sum")
     def total_sum(j):
         arrive(("fin_l", j))
         arrive(("fin_r", j))
@@ -376,14 +423,22 @@
         if 0 <= i - 6 < NCH:
             total_sum(i - 6)
 
-    for h in range(2):
+    @scoped("last_norm")
+    def last_norm(h):
         v = fs[0, 0, half(h), :].astype(F32) + macc[half(h), :]
         out[half(h), :] = normed(v, g2[...]).astype(BF16)
 
-    for copy in sent:
-        copy.wait_send()
-    for i in range(1, 8):
-        a2a_copy(i).wait_send()
+    for h in range(2):
+        last_norm(h)
+
+    @scoped("drain")
+    def drain():
+        for copy in sent:
+            copy.wait_send()
+        for i in range(1, 8):
+            a2a_copy(i).wait_send()
+
+    drain()
 
 
 def per_device(q, kv, sink, doc, stream, ow, g1, up, dn, g2):

time: 86.6 us -> 75.1 us (0.87)
  Pallas kernels: 84.5 us -> 73.1 us
    pallas_call x1, Pallas kernels: 84.5 us -> 73.1 us  [per_device(): pl.pallas_call(kernel, out_shape=jax.ShapeDtypeStruct(stream.shape, BF16)...]
where the time goes in v2:
time: 75.1 us; the launch traced here: 75 us
  Pallas kernels  73.1 us (97%)
  local copies, waits for them, and re-layouts  1.88 us (3%)
    pallas_call x1, Pallas kernels, per_device(): pl.pallas_call(kernel, out_shape=jax.ShapeDtypeStruct(stream.shape, BF16)...  73.1 us
    unnamed x1, local copies, waits for them, and re-layouts  1.88 us

profile of v2, /device:TPU:1, one launch (start us, length us, event | category | flops | bytes accessed | tf_op | source)
XLA Modules:
  0.0 75.0 jit_solution(16066390256672317891)
XLA Ops:
  0.0 73.1 %layer.1 = bf16[128,2048]{1,0:T(8,128)(2,1)} custom-call(bf16[1024,128]{1,0:T(8,128)(2,1)} %q_h.1, bf16[1024,128]{1,0:T(8,128)(2,1)} %bitcast.4, f32[2]{0:T(128)} %sink_s.1, s32[8,128]{1,0:T(8,128)} %bitcast.7, bf16[128,2048]{1,0:T(8,128)(2,1)} %st_h.1, bf16[1024,2048]{1,0:T(8,128)(2,1)} %ow_h.1, f32[1,2048]{1,0:T(1,128)} %bitcast.5, ...), custom_call_target="tpu_custom_call" | custom-call | tf_op jit(solution)/shard_map/layer/pallas_call | solution.py:447
  73.1 1.9 %copy.12 = bf16[128,2048]{1,0:T(8,128)(2,1)} copy(bf16[128,2048]{1,0:T(8,128)(2,1)} %layer.1) | data formatting | bytes 1048576

commit v3 on v2

--- a/solution.py
+++ b/solution.py
@@ -25,6 +25,21 @@
 ]
 RANK = {o: i for i, o in enumerate(ORDER)}
 
+AP, AM, BP, BM = (1, 0), (-1, 0), (0, 1), (0, -1)
+ONWARD = {
+    (3, 0): [(AP, 0), (BP, None), (BM, None)],
+    (1, 0): [(AM, 1), (BP, None), (BM, None)],
+    (2, 0): [(BP, None), (BM, None)],
+    (0, 3): [(BP, None)],
+    (3, 1): [(BM, None)],
+    (1, 3): [(BP, 0)],
+    (1, 1): [(BM, 1)],
+    (2, 3): [(BP, 0)],
+    (2, 1): [(BM, 1)],
+}
+HALVED = ((2, 0), (1, 2), (2, 2))
+KA = HID
+
 
 def nt_dot(a, b):
     return lax.dot_general(a, b, (((1,), (1,)), ((), ())), preferred_element_type=F32)
@@ -34,11 +49,10 @@
     return jnp.dot(a, b, preferred_element_type=F32)
 
 
-def normed(x, gain):
+def moments(x):
     centre = jnp.mean(x, axis=-1, keepdims=True)
     shifted = x - centre
-    spread = jnp.mean(shifted * shifted, axis=-1, keepdims=True)
-    return shifted * lax.rsqrt(spread + NORM_EPS) * gain
+    return centre, lax.rsqrt(jnp.mean(shifted * shifted, axis=-1, keepdims=True) + NORM_EPS)
 
 
 def scoped(name):
@@ -65,9 +79,9 @@
 
 
 def kernel(
-    q_h, kv_h, sink_s, doc_h, st_h, ow_h, g1, up_h, dn_h, g2, out,
-    qv, kvx, docv, doc_l, doc_r, docx, stv, owv, att_own, att_all, xbuf,
-    up_all, dn_all, fs, act, psend, prx, pown, s1, s2, s3, mid_l, mid_r, fin_l, fin_r, macc,
+    q_h, kv_h, sink_s, doc_h, st_h, ow_h, g1_h, up_h, dn_h, g2_h, out,
+    g1, g2, qv, kvx, docv, doc_l, doc_r, docx, stv, owv, att_own, att_all, xbuf,
+    up_all, dn_all, fs, hacc, act, psend, prx, pown, s1, s2, s3, mid_l, mid_r, fin_l, fin_r, macc,
     ss, rs, ls,
 ):
     sp, tp = lax.axis_index("sp"), lax.axis_index("tp")
@@ -85,16 +99,17 @@
     left = (sp, ((x + R - 1) % R) * 2 + core)
     sp_next, sp_prev = (sp + 1) % 16, (sp + 15) % 16
 
-    local_names = ["kv", "doc", "q", "up", "dn", "st", "ow"]
-    own_up = up_all.at[pl.ds(pl.multiple_of(sp * BLK, BLK), BLK), :]
+    local_names = ["kv", "doc", "up", "q", "st", "ow", "dn", "g1", "g2"]
     pairs = {
         "kv": (kv_h, kvx.at[pl.ds(BLK, 1024), :]),
         "doc": (doc_h, docv),
         "q": (q_h, qv),
-        "up": (up_h, own_up),
+        "up": (up_h, up_all.at[pl.ds(0, BLK), :]),
         "dn": (dn_h, dn_all.at[:, pl.ds(0, BLK)]),
         "st": (st_h, stv),
         "ow": (ow_h, owv),
+        "g1": (g1_h, g1),
+        "g2": (g2_h, g2),
     }
     local = {n: pltpu.make_async_copy(*pairs[n], ls.at[i]) for i, n in enumerate(local_names)}
     for n in local_names:
@@ -135,15 +150,14 @@
     send("doc_r", docv, doc_r, (sp_prev, tp))
 
     def block(w, origin, at, half):
-        da, db = origin
+        ra, rb = (origin[0] - at[0]) % R, (origin[1] - at[1]) % R
+        r0, r1 = RANK[(ra, rb)], RANK[(rb, ra)]
+        slot = (r0 + core * (r1 - r0)) * BLK
+        size = BLK if w == "u" else HID
+        lo, n = {None: (0, size), 0: (0, size // 2), 1: (size // 2, size // 2)}[half]
         if w == "u":
-            lo, n = {None: (0, BLK), 0: (0, BLK // 2), 1: (BLK // 2, BLK // 2)}[half]
-            return up_all.at[pl.ds(pl.multiple_of(sp_of(da, db) * BLK + lo, BLK // 2), n), :]
-        lo, n = {None: (0, HID), 0: (0, HID // 2), 1: (HID // 2, HID // 2)}[half]
-        ra, rb = (da - at[0]) % R, (db - at[1]) % R
-        r0, r1 = RANK[(ra, rb)], RANK[(rb, ra)]
-        slot = r0 + core * (r1 - r0)
-        return dn_all.at[pl.ds(lo, n), pl.ds(pl.multiple_of(slot * BLK, BLK), BLK)]
+            return up_all.at[pl.ds(pl.multiple_of(slot + lo, BLK // 2), n), :]
+        return dn_all.at[pl.ds(lo, n), pl.ds(pl.multiple_of(slot, BLK), BLK)]
 
     def pass_on(w, origin, to, half=None):
         rel = ((origin[0] - to[0]) % R, (origin[1] - to[1]) % R)
@@ -152,7 +166,6 @@
             (sp_of(to[0] % R, to[1] % R), tp),
         )
 
-    AP, AM, BP, BM = (1, 0), (-1, 0), (0, 1), (0, -1)
     relayed = set()
 
     @scoped("need")
@@ -160,35 +173,21 @@
         if (w, origin) in relayed:
             return
         relayed.add((w, origin))
-        if origin == (2, 0):
-            arrive((w, origin, 0))
-            arrive((w, origin, 1))
-        else:
-            arrive((w, origin, None))
-        if origin == (3, 0):
-            pass_on(w, origin, AP, 0)
-        if origin == (1, 0):
-            pass_on(w, origin, AM, 1)
-        if origin in ((3, 0), (1, 0), (2, 0)):
-            pass_on(w, origin, BP)
-            pass_on(w, origin, BM)
-        if origin in ((0, 3), (2, 3)):
-            pass_on(w, origin, BP)
-        if origin in ((3, 1), (1, 1)):
-            pass_on(w, origin, BM)
-        if (w, origin) == ("u", (1, 1)):
-            local["dn"].wait()
-            pass_on("d", (0, 0), BP)
-            pass_on("d", (0, 0), BM)
-        if (w, origin) == ("u", (2, 3)):
-            pass_on("d", (0, 0), AP)
-            pass_on("d", (0, 0), AM)
+        for h in (0, 1) if origin in HALVED else (None,):
+            arrive((w, origin, h))
+        for to, h in ONWARD.get(origin, ()):
+            pass_on(w, origin, to, h)
+
+    def own_down(*ways):
+        for to in ways:
+            pass_on("d", (0, 0), to)
 
     local["up"].wait()
     for to in (AP, AM):
         pass_on("u", (0, 0), to)
 
     local["q"].wait()
+    local["dn"].wait()
     docx[pl.ds(8, 8), :] = docv[...].astype(F32)
     row = lax.broadcasted_iota(jnp.int32, (BLK, BLK), 0)
     col = lax.broadcasted_iota(jnp.int32, (BLK, BLK), 1)
@@ -266,8 +265,6 @@
         return carry
 
     lax.fori_loop(0, 1, outer, 0)
-    need("u", (3, 0))
-    need("u", (1, 0))
 
     def a2a_copy(i):
         other = (tp + i) % 8
@@ -282,9 +279,12 @@
     def a2a_wait():
         local["ow"].wait()
         local["st"].wait()
+        local["g1"].wait()
         for i in range(1, 8):
             a2a_copy(i).wait_recv()
 
+    need("u", (3, 0))
+    need("u", (1, 0))
     a2a_wait()
 
     def project(n):
@@ -297,7 +297,10 @@
             project(n)
 
     projection()
-    need("u", (0, 3))
+
+    def cols_of(rank):
+        dy, dz = ORDER[rank]
+        return pl.ds(pl.multiple_of((((z + dz) % R) * R + (y + dy) % R) * BLK, BLK), BLK)
 
     HALF = BLK // 2
     half = lambda h: pl.ds(h * HALF, HALF)
@@ -307,7 +310,11 @@
 
     @scoped("first_norm")
     def first_norm(h):
-        fs[0, 0, half(h), :] = normed(xbuf[half(h), :], g1[...]).astype(BF16)
+        centre, factor = moments(xbuf[half(h), :])
+        for r in range(16):
+            c = cols_of(r)
+            v = (xbuf[half(h), c] - centre) * factor * g1[:, c]
+            fs[0, 0, half(h), pl.ds(r * BLK, BLK)] = v.astype(BF16)
 
     for h in range(2):
         first_norm(h)
@@ -333,54 +340,47 @@
         elif name == "x_2":
             fs_send("c2", (0, 2), (1, 2), h, partner)
 
+    def needs(w, ranks):
+        for o in ranks:
+            for origin in (o, (o[1], o[0])):
+                if origin != (0, 0):
+                    need(w, origin)
+
+    @scoped("hidden_a")
+    def hidden_a(dx):
+        for h in range(2):
+            arrive((f"c{dx}", h))
+        needs("u", ORDER[: KA // BLK])
+        for n in range(HID // 256):
+            cols = pl.ds(n * 256, 256)
+            rows = fs[:, dx, :, 0:KA].reshape(2 * BLK, KA)
+            hacc[min(dx, 2), :, cols] = dot(rows, up_all[0:KA, cols])
+
     @scoped("hidden")
     def hidden(dx):
         for h in range(2):
             arrive((f"c{dx}", h))
-
+        needs("u", ORDER)
+        lo = 0 if dx == 2 else KA
         for n in range(HID // 256):
             cols = pl.ds(n * 256, 256)
-            rows = fs[:, dx].reshape(2 * BLK, D)
-            v = jnp.maximum(dot(rows, up_all[:, cols]), 0.0)
+            rows = fs[:, dx, :, lo:D].reshape(2 * BLK, D - lo)
+            v = dot(rows, up_all[lo:D, cols])
+            if lo:
+                v = v + hacc[min(dx, 2), :, cols]
+            v = jnp.maximum(v, 0.0)
             act[:, dx, :, cols] = (v * v).astype(BF16).reshape(2, BLK, 256)
 
-    need("u", (2, 0))
-    need("u", (3, 1))
-    need("u", (1, 1))
-    gather_rows("x_l", 0)
-    gather_rows("x_r", 1)
-    need("u", (2, 3))
-    gather_rows("x_l", 1)
-    gather_rows("x_r", 0)
-    need("d", (0, 3))
-    need("d", (3, 0))
-    need("d", (1, 0))
-    gather_rows("x_2", 0)
-    gather_rows("x_2", 1)
-    for da in range(R):
-        for db in range(R):
-            if (da, db) != (0, 0):
-                need("u", (da, db))
-    hidden(0)
-    hidden(1)
-    need("d", (2, 0))
-    hidden(3)
-    need("d", (3, 1))
-    hidden(2)
-
-    def cols_of(rank):
-        dy, dz = ORDER[rank]
-        return pl.ds(pl.multiple_of((((z + dz) % R) * R + (y + dy) % R) * BLK, BLK), BLK)
-
-    @scoped("product")
-    def product(j):
-        for o in (ORDER[2 * j], ORDER[2 * j + 1]):
-            for origin in (o, (o[1], o[0])):
-                if origin != (0, 0):
-                    need("d", origin)
+    @scoped("product_a")
+    def product_a(j):
+        needs("d", ORDER[2 * j : 2 * j + 2])
         cols = pl.ds(j * CW, CW)
         psend[j] = dot(act[1].reshape(4 * BLK, HID), dn_all[:, cols]).astype(BF16).reshape(R, BLK, CW)
         send(("p", j), psend.at[j], prx.at[j], partner)
+
+    @scoped("product_b")
+    def product_b(j):
+        cols = pl.ds(j * CW, CW)
         pown[j] = dot(act[0].reshape(4 * BLK, HID), dn_all[:, cols]).reshape(R, BLK, CW)
 
     @scoped("pair_sum")
@@ -389,9 +389,7 @@
         s2[j] = (pown[j, 2] + prx[j, 2].astype(F32)).astype(BF16)
         send(("mid_l", j), s2.at[j, pl.ds(0, HALF), :], mid_l.at[j], right)
         send(("mid_r", j), s2.at[j, pl.ds(HALF, HALF), :], mid_r.at[j], left)
-        mine = pown[j, 0] + prx[j, 0].astype(F32)
-        for i in range(2):
-            macc[:, cols_of(2 * j + i)] = mine[:, i * BLK : (i + 1) * BLK]
+        macc[:, pl.ds(j * CW, CW)] = pown[j, 0] + prx[j, 0].astype(F32)
 
     @scoped("middle")
     def middle(j):
@@ -409,25 +407,89 @@
     def total_sum(j):
         arrive(("fin_l", j))
         arrive(("fin_r", j))
-        v = fin_l[j].astype(F32) + fin_r[j].astype(F32)
-        for i in range(2):
-            macc[:, cols_of(2 * j + i)] += v[:, i * BLK : (i + 1) * BLK]
-
-    for i in range(NCH + 6):
-        if i < NCH:
-            product(i)
-        if 0 <= i - 1 < NCH:
-            pair_sum(i - 1)
-        if 0 <= i - 3 < NCH:
-            middle(i - 3)
-        if 0 <= i - 6 < NCH:
-            total_sum(i - 6)
-
+        macc[:, pl.ds(j * CW, CW)] += fin_l[j].astype(F32) + fin_r[j].astype(F32)
+
+    need("u", (0, 3))
+    need("u", (2, 0))
+    need("u", (3, 1))
+    need("u", (1, 3))
+    need("u", (1, 1))
+    hidden_a(0)
+    gather_rows("x_l", 0)
+    gather_rows("x_r", 1)
+    need("u", (2, 1))
+    need("u", (2, 3))
+    own_down(AP, AM)
+    own_down(BP, BM)
+    gather_rows("x_l", 1)
+    gather_rows("x_r", 0)
+    hidden_a(3)
+    hidden_a(1)
+    hidden(0)
+    hidden(1)
+    hidden(3)
+    gather_rows("x_2", 0)
+    gather_rows("x_2", 1)
+    need("d", (3, 0))
+    need("d", (1, 0))
+    hidden(2)
+    need("d", (0, 3))
+    product_a(0)
+    product_b(0)
+    product_a(1)
+    need("d", (2, 0))
+    product_b(1)
+    pair_sum(0)
+    need("d", (3, 1))
+    product_a(2)
+    pair_sum(1)
+    product_b(2)
+    middle(0)
+    pair_sum(2)
+    need("d", (1, 3))
+    need("d", (1, 1))
+    product_a(3)
+    middle(1)
+    product_b(3)
+    pair_sum(3)
+    total_sum(0)
+    need("d", (2, 1))
+    product_a(4)
+    middle(2)
+    product_b(4)
+    total_sum(1)
+    pair_sum(4)
+    middle(3)
+    need("d", (2, 3))
+    product_a(5)
+    product_b(5)
+    total_sum(2)
+    product_a(6)
+    pair_sum(5)
+    middle(4)
+    product_b(6)
+    product_a(7)
+    total_sum(3)
+    pair_sum(6)
+    product_b(7)
+    middle(5)
+    pair_sum(7)
+    total_sum(4)
+    middle(6)
+    total_sum(5)
+    middle(7)
+    total_sum(6)
+    total_sum(7)
     @scoped("last_norm")
     def last_norm(h):
-        v = fs[0, 0, half(h), :].astype(F32) + macc[half(h), :]
-        out[half(h), :] = normed(v, g2[...]).astype(BF16)
-
+        macc[half(h), :] += fs[0, 0, half(h), :].astype(F32)
+        centre, factor = moments(macc[half(h), :])
+        for r in range(16):
+            c = cols_of(r)
+            v = (macc[half(h), pl.ds(r * BLK, BLK)] - centre) * factor * g2[:, c]
+            out[half(h), c] = v.astype(BF16)
+
+    local["g2"].wait()
     for h in range(2):
         last_norm(h)
 
@@ -441,15 +503,21 @@
     drain()
 
 
+def far(v):
+    return pltpu.with_memory_space_constraint(v, pltpu.HBM)
+
+
 def per_device(q, kv, sink, doc, stream, ow, g1, up, dn, g2):
     vm, anyw = pl.BlockSpec(memory_space=pltpu.VMEM), pl.BlockSpec(memory_space=pl.ANY)
     smem = pl.BlockSpec(memory_space=pltpu.SMEM)
     return pl.pallas_call(
         kernel,
         out_shape=jax.ShapeDtypeStruct(stream.shape, BF16),
-        in_specs=[anyw, anyw, smem, anyw, anyw, anyw, vm, anyw, anyw, vm],
+        in_specs=[anyw, anyw, smem, anyw, anyw, anyw, anyw, anyw, anyw, anyw],
         out_specs=vm,
         scratch_shapes=[
+            pltpu.VMEM((1, D), F32),
+            pltpu.VMEM((1, D), F32),
             pltpu.VMEM((1024, BLK), BF16),
             pltpu.VMEM((1024 + 2 * BLK, BLK), BF16),
             pltpu.VMEM((8, BLK), jnp.int32),
@@ -464,6 +532,7 @@
             pltpu.VMEM((D, HID), BF16),
             pltpu.VMEM((HID, D), BF16),
             pltpu.VMEM((2, R, BLK, D), BF16),
+            pltpu.VMEM((3, 2 * BLK, HID), F32),
             pltpu.VMEM((2, R, BLK, HID), BF16),
             pltpu.VMEM((NCH, R, BLK, CW), BF16),
             pltpu.VMEM((NCH, R, BLK, CW), BF16),
@@ -478,14 +547,15 @@
             pltpu.VMEM((BLK, D), F32),
             pltpu.SemaphoreType.DMA((112,)),
             pltpu.SemaphoreType.DMA((112,)),
-            pltpu.SemaphoreType.DMA((8,)),
+            pltpu.SemaphoreType.DMA((9,)),
         ],
         compiler_params=pltpu.CompilerParams(
-            collective_id=0, has_side_effects=True, vmem_limit_bytes=60 * 1024 * 1024
+            collective_id=0, has_side_effects=True, vmem_limit_bytes=48 * 1024 * 1024
         ),
         name="layer",
     )(
-        q, kv.reshape(1024, BLK), sink, doc.reshape(8, BLK), stream, ow, g1.reshape(1, D), up, dn, g2.reshape(1, D)
+        far(q), far(kv.reshape(1024, BLK)), far(sink), far(doc.reshape(8, BLK)), far(stream), far(ow),
+        far(g1.reshape(1, D)), far(up), far(dn), far(g2.reshape(1, D)),
     )
 
 

time: 75.1 us -> 72.3 us (0.963)
  Pallas kernels: 73.1 us -> 70.8 us
  local copies, waits for them, and re-layouts: 1.88 us -> 0.8 us
    pallas_call x1, Pallas kernels: 73.1 us -> 70.8 us  [per_device(): pl.pallas_call(kernel, out_shape=jax.ShapeDtypeStruct(stream.shape, BF16)...]
    unnamed x1, local copies, waits for them, and re-layouts: 1.88 us -> 0.8 us
where the time goes in v3:
time: 72.3 us; the launch traced here: 71.6 us
  Pallas kernels  70.8 us (98%)
  local copies, waits for them, and re-layouts  0.8 us (1%)
    pallas_call x1, Pallas kernels, per_device(): pl.pallas_call(kernel, out_shape=jax.ShapeDtypeStruct(stream.shape, BF16)...  70.8 us

profile of v3, /device:TPU:1, one launch (start us, length us, event | category | flops | bytes accessed | tf_op | source)
XLA Modules:
  0.0 71.6 jit_solution(727255995343662775)
XLA Ops:
  0.0 70.8 %layer.1 = bf16[128,2048]{1,0:T(8,128)(2,1)S(1)} custom-call(bf16[1024,128]{1,0:T(8,128)(2,1)} %q_h.1, bf16[1024,128]{1,0:T(8,128)(2,1)} %bitcast.4, f32[2]{0:T(128)} %sink_s.1, s32[8,128]{1,0:T(8,128)} %bitcast.7, bf16[128,2048]{1,0:T(8,128)(2,1)} %st_h.1, bf16[1024,2048]{1,0:T(8,128)(2,1)} %ow_h.1, f32[1,2048]{1,0:T(1,128)} %bitcast.5, ...), custom_call_target="tpu_custom_call" | custom-call | tf_op jit(solution)/shard_map/layer/pallas_call | solution.py:513
  70.8 0.8 %copy.12 = bf16[128,2048]{1,0:T(8,128)(2,1)} copy(bf16[128,2048]{1,0:T(8,128)(2,1)S(1)} %layer.1) | data formatting | bytes 1048576

commit v4 on v3

--- a/solution.py
+++ b/solution.py
@@ -30,14 +30,14 @@
     (3, 0): [(AP, 0), (BP, None), (BM, None)],
     (1, 0): [(AM, 1), (BP, None), (BM, None)],
     (2, 0): [(BP, None), (BM, None)],
-    (0, 3): [(BP, None)],
-    (3, 1): [(BM, None)],
-    (1, 3): [(BP, 0)],
-    (1, 1): [(BM, 1)],
+    (0, 3): [(BP, 0)],
+    (0, 1): [(BM, 1)],
+    (3, 3): [(BP, None)],
+    (1, 1): [(BM, None)],
     (2, 3): [(BP, 0)],
     (2, 1): [(BM, 1)],
 }
-HALVED = ((2, 0), (1, 2), (2, 2))
+HALVED = ((2, 0), (0, 2), (2, 2))
 KA = HID
 
 
@@ -99,6 +99,12 @@
     left = (sp, ((x + R - 1) % R) * 2 + core)
     sp_next, sp_prev = (sp + 1) % 16, (sp + 15) % 16
 
+    barrier = pltpu.get_barrier_semaphore()
+    greet = [(sp, (tp + i) % 8) for i in range(1, 8)]
+    greet += [(sp_of(da, db), tp) for da, db in ((1, 0), (3, 0), (0, 1), (0, 3))]
+    greet += [(sp_next, tp), (sp_prev, tp)]
+    for dev in greet:
+        pl.semaphore_signal(barrier, inc=1, device_id=dev, device_id_type=MESH)
     local_names = ["kv", "doc", "up", "q", "st", "ow", "dn", "g1", "g2"]
     pairs = {
         "kv": (kv_h, kvx.at[pl.ds(BLK, 1024), :]),
@@ -115,12 +121,6 @@
     for n in local_names:
         local[n].start()
 
-    barrier = pltpu.get_barrier_semaphore()
-    greet = [(sp, (tp + i) % 8) for i in range(1, 8)]
-    greet += [(sp_of(da, db), tp) for da, db in ((1, 0), (3, 0), (0, 1), (0, 3))]
-    greet += [(sp_next, tp), (sp_prev, tp)]
-    for dev in greet:
-        pl.semaphore_signal(barrier, inc=1, device_id=dev, device_id_type=MESH)
     pl.semaphore_wait(barrier, len(greet))
 
     sems = Sems()
@@ -185,9 +185,10 @@
     local["up"].wait()
     for to in (AP, AM):
         pass_on("u", (0, 0), to)
+    local["dn"].wait()
+    own_down(AP, AM)
 
     local["q"].wait()
-    local["dn"].wait()
     docx[pl.ds(8, 8), :] = docv[...].astype(F32)
     row = lax.broadcasted_iota(jnp.int32, (BLK, BLK), 0)
     col = lax.broadcasted_iota(jnp.int32, (BLK, BLK), 1)
@@ -283,8 +284,6 @@
         for i in range(1, 8):
             a2a_copy(i).wait_recv()
 
-    need("u", (3, 0))
-    need("u", (1, 0))
     a2a_wait()
 
     def project(n):
@@ -305,8 +304,9 @@
     HALF = BLK // 2
     half = lambda h: pl.ds(h * HALF, HALF)
 
-    def fs_send(name, src, dst, h, dev):
-        send((name, h), fs.at[src[0], src[1], half(h), :], fs.at[dst[0], dst[1], half(h), :], dev)
+    def fs_send(name, src, dst, i, dev, n=HALF):
+        rows = pl.ds(i * n, n)
+        send((name, i), fs.at[src[0], src[1], rows, :], fs.at[dst[0], dst[1], rows, :], dev)
 
     @scoped("first_norm")
     def first_norm(h):
@@ -329,16 +329,14 @@
     @scoped("gather_rows")
     def gather_rows(name, h):
         arrive((name, h))
-        if name == "x_l":
-            if h == 0:
-                fs_send("x_2", (0, 3), (0, 2), 0, right)
-            fs_send("c3", (0, 3), (1, 3), h, partner)
-        elif name == "x_r":
-            if h == 1:
-                fs_send("x_2", (0, 1), (0, 2), 1, left)
-            fs_send("c1", (0, 1), (1, 1), h, partner)
-        elif name == "x_2":
-            fs_send("c2", (0, 2), (1, 2), h, partner)
+        if name == "x_2":
+            fs_send("c2", (0, 2), (1, 2), h, partner, BLK // 4)
+            return
+        slot, onward, first = (3, right, 0) if name == "x_l" else (1, left, 1)
+        if h == first:
+            for q in (2 * h, 2 * h + 1):
+                fs_send("x_2", (0, slot), (0, 2), q, onward, BLK // 4)
+        fs_send(f"c{slot}", (0, slot), (1, slot), h, partner)
 
     def needs(w, ranks):
         for o in ranks:
@@ -358,8 +356,8 @@
 
     @scoped("hidden")
     def hidden(dx):
-        for h in range(2):
-            arrive((f"c{dx}", h))
+        for i in range(4 if dx == 2 else 2):
+            arrive((f"c{dx}", i))
         needs("u", ORDER)
         lo = 0 if dx == 2 else KA
         for n in range(HID // 256):
@@ -383,101 +381,110 @@
         cols = pl.ds(j * CW, CW)
         pown[j] = dot(act[0].reshape(4 * BLK, HID), dn_all[:, cols]).reshape(R, BLK, CW)
 
+    LO, HI = pl.ds(0, HALF), pl.ds(HALF, HALF)
+
+    def pair(j, dx, rows=slice(None)):
+        return pown[j, dx, rows, :] + prx[j, dx, rows, :].astype(F32)
+
     @scoped("pair_sum")
     def pair_sum(j):
         arrive(("p", j))
-        s2[j] = (pown[j, 2] + prx[j, 2].astype(F32)).astype(BF16)
-        send(("mid_l", j), s2.at[j, pl.ds(0, HALF), :], mid_l.at[j], right)
-        send(("mid_r", j), s2.at[j, pl.ds(HALF, HALF), :], mid_r.at[j], left)
-        macc[:, pl.ds(j * CW, CW)] = pown[j, 0] + prx[j, 0].astype(F32)
+        s2[j] = pair(j, 2).astype(BF16)
+        send(("mid_l", j), s2.at[j, LO, :], mid_l.at[j], right)
+        send(("mid_r", j), s2.at[j, HI, :], mid_r.at[j], left)
+        s1[j, HI, :] = pair(j, 1, HI).astype(BF16)
+        s3[j, LO, :] = pair(j, 3, LO).astype(BF16)
+        send(("dir_l", j), s1.at[j, HI, :], fin_l.at[j, HI, :], right)
+        send(("dir_r", j), s3.at[j, LO, :], fin_r.at[j, LO, :], left)
+        macc[:, pl.ds(j * CW, CW)] = pair(j, 0)
 
     @scoped("middle")
     def middle(j):
-        lo, hi = pl.ds(0, HALF), pl.ds(HALF, HALF)
-        s1[j, hi, :] = (pown[j, 1, hi, :] + prx[j, 1, hi, :].astype(F32)).astype(BF16)
-        s3[j, lo, :] = (pown[j, 3, lo, :] + prx[j, 3, lo, :].astype(F32)).astype(BF16)
         arrive(("mid_l", j))
-        s1[j, lo, :] = (pown[j, 1, lo, :] + prx[j, 1, lo, :].astype(F32) + mid_l[j].astype(F32)).astype(BF16)
-        send(("fin_l", j), s1.at[j], fin_l.at[j], right)
+        s1[j, LO, :] = (pair(j, 1, LO) + mid_l[j].astype(F32)).astype(BF16)
+        send(("fin_l", j), s1.at[j, LO, :], fin_l.at[j, LO, :], right)
         arrive(("mid_r", j))
-        s3[j, hi, :] = (pown[j, 3, hi, :] + prx[j, 3, hi, :].astype(F32) + mid_r[j].astype(F32)).astype(BF16)
-        send(("fin_r", j), s3.at[j], fin_r.at[j], left)
+        s3[j, HI, :] = (pair(j, 3, HI) + mid_r[j].astype(F32)).astype(BF16)
+        send(("fin_r", j), s3.at[j, HI, :], fin_r.at[j, HI, :], left)
 
     @scoped("total_sum")
     def total_sum(j):
-        arrive(("fin_l", j))
-        arrive(("fin_r", j))
+        for name in ("dir_l", "dir_r", "fin_l", "fin_r"):
+            arrive((name, j))
         macc[:, pl.ds(j * CW, CW)] += fin_l[j].astype(F32) + fin_r[j].astype(F32)
 
+    need("u", (3, 0))
+    need("u", (1, 0))
     need("u", (0, 3))
+    need("u", (0, 1))
     need("u", (2, 0))
-    need("u", (3, 1))
-    need("u", (1, 3))
+    need("u", (3, 3))
+    gather_rows("x_l", 0)
+    gather_rows("x_r", 1)
     need("u", (1, 1))
     hidden_a(0)
-    gather_rows("x_l", 0)
-    gather_rows("x_r", 1)
-    need("u", (2, 1))
-    need("u", (2, 3))
-    own_down(AP, AM)
-    own_down(BP, BM)
     gather_rows("x_l", 1)
     gather_rows("x_r", 0)
+    need("u", (2, 3))
+    need("u", (2, 1))
+    own_down(BP, BM)
+    need("d", (3, 0))
+    need("d", (1, 0))
     hidden_a(3)
     hidden_a(1)
+    gather_rows("x_2", 0)
+    gather_rows("x_2", 2)
+    need("d", (2, 0))
+    gather_rows("x_2", 1)
+    gather_rows("x_2", 3)
     hidden(0)
     hidden(1)
     hidden(3)
-    gather_rows("x_2", 0)
-    gather_rows("x_2", 1)
-    need("d", (3, 0))
-    need("d", (1, 0))
     hidden(2)
     need("d", (0, 3))
+    need("d", (0, 1))
     product_a(0)
     product_b(0)
     product_a(1)
-    need("d", (2, 0))
+    need("d", (3, 3))
     product_b(1)
     pair_sum(0)
-    need("d", (3, 1))
     product_a(2)
+    product_b(2)
     pair_sum(1)
-    product_b(2)
-    middle(0)
-    pair_sum(2)
-    need("d", (1, 3))
     need("d", (1, 1))
     product_a(3)
+    pair_sum(2)
+    middle(0)
+    product_b(3)
     middle(1)
-    product_b(3)
     pair_sum(3)
+    need("d", (2, 3))
+    need("d", (2, 1))
+    middle(2)
+    product_a(4)
     total_sum(0)
-    need("d", (2, 1))
-    product_a(4)
-    middle(2)
     product_b(4)
     total_sum(1)
+    middle(3)
     pair_sum(4)
-    middle(3)
-    need("d", (2, 3))
     product_a(5)
+    total_sum(2)
     product_b(5)
-    total_sum(2)
     product_a(6)
+    total_sum(3)
+    product_b(6)
     pair_sum(5)
     middle(4)
-    product_b(6)
     product_a(7)
-    total_sum(3)
     pair_sum(6)
     product_b(7)
+    pair_sum(7)
     middle(5)
-    pair_sum(7)
     total_sum(4)
     middle(6)
+    middle(7)
     total_sum(5)
-    middle(7)
     total_sum(6)
     total_sum(7)
     @scoped("last_norm")
@@ -545,8 +552,8 @@
             pltpu.VMEM((NCH, BLK, CW), BF16),
             pltpu.VMEM((NCH, BLK, CW), BF16),
             pltpu.VMEM((BLK, D), F32),
-            pltpu.SemaphoreType.DMA((112,)),
-            pltpu.SemaphoreType.DMA((112,)),
+            pltpu.SemaphoreType.DMA((128,)),
+            pltpu.SemaphoreType.DMA((128,)),
             pltpu.SemaphoreType.DMA((9,)),
         ],
         compiler_params=pltpu.CompilerParams(

time: 72.3 us -> 69.5 us (0.961)
  Pallas kernels: 70.8 us -> 68.6 us
    pallas_call x1, Pallas kernels: 70.8 us -> 68.6 us  [per_device(): pl.pallas_call(kernel, out_shape=jax.ShapeDtypeStruct(stream.shape, BF16)...]
where the time goes in v4:
time: 69.5 us; the launch traced here: 69.4 us
  Pallas kernels  68.6 us (99%)
  local copies, waits for them, and re-layouts  0.8 us (1%)
    pallas_call x1, Pallas kernels, per_device(): pl.pallas_call(kernel, out_shape=jax.ShapeDtypeStruct(stream.shape, BF16)...  68.6 us

profile of v4, /device:TPU:1, one launch (start us, length us, event | category | flops | bytes accessed | tf_op | source)
XLA Modules:
  0.0 69.4 jit_solution(17166027812321226726)
XLA Ops:
  0.0 68.6 %layer.1 = bf16[128,2048]{1,0:T(8,128)(2,1)S(1)} custom-call(bf16[1024,128]{1,0:T(8,128)(2,1)} %q_h.1, bf16[1024,128]{1,0:T(8,128)(2,1)} %bitcast.4, f32[2]{0:T(128)} %sink_s.1, s32[8,128]{1,0:T(8,128)} %bitcast.7, bf16[128,2048]{1,0:T(8,128)(2,1)} %st_h.1, bf16[1024,2048]{1,0:T(8,128)(2,1)} %ow_h.1, f32[1,2048]{1,0:T(1,128)} %bitcast.5, ...), custom_call_target="tpu_custom_call" | custom-call | tf_op jit(solution)/shard_map/layer/pallas_call | solution.py:520
  68.6 0.8 %copy.12 = bf16[128,2048]{1,0:T(8,128)(2,1)} copy(bf16[128,2048]{1,0:T(8,128)(2,1)S(1)} %layer.1) | data formatting | bytes 1048576

commit v5 on v4

--- a/solution.py
+++ b/solution.py
@@ -18,6 +18,7 @@
 HID = 1024
 NCH = 8
 CW = D // NCH
+SENDS, ARRIVALS = 13, 65
 
 ORDER = [
     (0, 0), (1, 0), (3, 0), (0, 1), (0, 3), (3, 3), (3, 1), (1, 1),
@@ -37,7 +38,7 @@
     (2, 3): [(BP, 0)],
     (2, 1): [(BM, 1)],
 }
-HALVED = ((2, 0), (0, 2), (2, 2))
+TOGETHER = (((3, 1), (1, 3)), ((0, 2), (3, 2), (1, 2), (2, 2)))
 KA = HID
 
 
@@ -72,16 +73,14 @@
     def __init__(self):
         self.index = {}
 
-    def at(self, key, count=1):
-        if key not in self.index:
-            self.index[key] = (sum(c for _, c in self.index.values()), count)
-        return self.index[key][0]
+    def at(self, key):
+        return self.index.setdefault(key, len(self.index))
 
 
 def kernel(
     q_h, kv_h, sink_s, doc_h, st_h, ow_h, g1_h, up_h, dn_h, g2_h, out,
-    g1, g2, qv, kvx, docv, doc_l, doc_r, docx, stv, owv, att_own, att_all, xbuf,
-    up_all, dn_all, fs, hacc, act, psend, prx, pown, s1, s2, s3, mid_l, mid_r, fin_l, fin_r, macc,
+    g1, g2, qv, kvx, docv, doc_lr, docx, stv, owv, att_own, att_all, xbuf,
+    up_all, dn_all, fs, hacc, act, psend, prx, pown, s1, s2, s3, mid, fin, macc,
     ss, rs, ls,
 ):
     sp, tp = lax.axis_index("sp"), lax.axis_index("tp")
@@ -123,31 +122,39 @@
 
     pl.semaphore_wait(barrier, len(greet))
 
-    sems = Sems()
-    sent = []
+    send_sems, recv_sems = Sems(), Sems()
+    ends = {}
     waited = set()
-    arriving = {}
-
-    def send(key, src, dst, dev):
-        i = sems.at(key)
+
+    def send(key, src, dst, dev, group, whole, with_key=None, with_dst=None):
+        pltpu.make_async_remote_copy(
+            src_ref=src, dst_ref=dst, send_sem=ss.at[send_sems.at(group)],
+            recv_sem=rs.at[recv_sems.at(with_key or key)], device_id=dev, device_id_type=MESH,
+        ).start()
+        ends[("s", group)] = whole
+        ends[("r", with_key or key)] = dst if with_dst is None else with_dst
+
+    def wait(kind, key):
+        ref = ends[(kind, key)]
+        i = (send_sems if kind == "s" else recv_sems).at(key)
         copy = pltpu.make_async_remote_copy(
-            src_ref=src, dst_ref=dst, send_sem=ss.at[i], recv_sem=rs.at[i], device_id=dev, device_id_type=MESH
+            src_ref=ref, dst_ref=ref, send_sem=ss.at[i], recv_sem=rs.at[i], device_id=partner, device_id_type=MESH
         )
-        copy.start()
-        sent.append(copy)
-        arriving[key] = copy
+        copy.wait_send() if kind == "s" else copy.wait_recv()
 
     def arrive(key):
         if key not in waited:
             waited.add(key)
-            arriving[key].wait_recv()
+            wait("r", key)
 
     local["kv"].wait()
     local["doc"].wait()
-    send("kv_l", kvx.at[pl.ds(1024, BLK), :], kvx.at[pl.ds(0, BLK), :], (sp_next, tp))
-    send("kv_r", kvx.at[pl.ds(BLK, BLK), :], kvx.at[pl.ds(1024 + BLK, BLK), :], (sp_prev, tp))
-    send("doc_l", docv, doc_l, (sp_next, tp))
-    send("doc_r", docv, doc_r, (sp_prev, tp))
+    rim = kvx.at[pl.ds(0, 2 * BLK), :]
+    for src, dst, dev in ((1024, 0, sp_next), (BLK, 1024 + BLK, sp_prev)):
+        rows = kvx.at[pl.ds(src, BLK), :], kvx.at[pl.ds(dst, BLK), :]
+        send("kv", *rows, (dev, tp), "kv", rim, "kv", rim)
+    send("doc", docv, doc_lr.at[pl.ds(0, 8), :], (sp_next, tp), "doc", doc_lr, "doc", doc_lr)
+    send("doc", docv, doc_lr.at[pl.ds(8, 8), :], (sp_prev, tp), "doc", doc_lr, "doc", doc_lr)
 
     def block(w, origin, at, half):
         ra, rb = (origin[0] - at[0]) % R, (origin[1] - at[1]) % R
@@ -161,9 +168,14 @@
 
     def pass_on(w, origin, to, half=None):
         rel = ((origin[0] - to[0]) % R, (origin[1] - to[1]) % R)
+        held = up_all if w == "u" else dn_all
+        together = {o: g for g in TOGETHER for o in g}.get(rel, (rel,)) if w == "u" else (rel,)
+        n = len(together) * BLK
         send(
-            (w, rel, half), block(w, origin, (0, 0), half), block(w, origin, to, half),
+            (w, rel), block(w, origin, (0, 0), half), block(w, origin, to, half),
             (sp_of(to[0] % R, to[1] % R), tp),
+            w, held.at[pl.ds(0, 15 * BLK), :] if w == "u" else held.at[:, pl.ds(0, 15 * BLK)],
+            (w, together), held.at[pl.ds(0, n), :] if w == "u" else held.at[:, pl.ds(0, n)],
         )
 
     relayed = set()
@@ -173,8 +185,7 @@
         if (w, origin) in relayed:
             return
         relayed.add((w, origin))
-        for h in (0, 1) if origin in HALVED else (None,):
-            arrive((w, origin, h))
+        arrive((w, {o: g for g in TOGETHER for o in g}.get(origin, (origin,)) if w == "u" else (origin,)))
         for to, h in ONWARD.get(origin, ()):
             pass_on(w, origin, to, h)
 
@@ -193,7 +204,8 @@
     row = lax.broadcasted_iota(jnp.int32, (BLK, BLK), 0)
     col = lax.broadcasted_iota(jnp.int32, (BLK, BLK), 1)
     low = col < 64
-    a2a = sems.at("a2a", 8)
+    a2a_send, a2a_recv = send_sems.at("a2a"), recv_sems.at("a2a")
+    ends[("s", "a2a")] = ends[("r", "a2a")] = att_own.at[pl.ds(0, 7 * BLK), :]
 
     def attended(blk):
         rows = pl.ds(pl.multiple_of(blk * BLK, BLK), BLK)
@@ -232,7 +244,7 @@
         def _():
             pltpu.make_async_remote_copy(
                 src_ref=att_own.at[rows, :], dst_ref=att_all.at[:, mine],
-                send_sem=ss.at[a2a + blk], recv_sem=rs.at[a2a + tp],
+                send_sem=ss.at[a2a_send], recv_sem=rs.at[a2a_recv],
                 device_id=(sp, blk), device_id_type=MESH,
             ).start()
 
@@ -256,35 +268,27 @@
     for to in (BP, BM):
         pass_on("u", (0, 0), to)
     lax.fori_loop(2, 3, inner, 0)
-    for key in ("kv_l", "kv_r", "doc_l", "doc_r"):
-        arrive(key)
-    docx[pl.ds(0, 8), :] = jnp.where(sp == 0, -1.0, doc_l[...].astype(F32))
-    docx[pl.ds(16, 8), :] = jnp.where(sp == 15, -1.0, doc_r[...].astype(F32))
+    arrive("kv")
+    arrive("doc")
+    docx[pl.ds(0, 8), :] = jnp.where(sp == 0, -1.0, doc_lr[pl.ds(0, 8), :].astype(F32))
+    docx[pl.ds(16, 8), :] = jnp.where(sp == 15, -1.0, doc_lr[pl.ds(8, 8), :].astype(F32))
 
     def outer(i, carry):
         attend(i, i + 7)
         return carry
 
     lax.fori_loop(0, 1, outer, 0)
-
-    def a2a_copy(i):
-        other = (tp + i) % 8
-        return pltpu.make_async_remote_copy(
-            src_ref=att_own.at[pl.ds(pl.multiple_of(other * BLK, BLK), BLK), :],
-            dst_ref=att_all.at[:, pl.ds(pl.multiple_of(other * BLK, BLK), BLK)],
-            send_sem=ss.at[a2a + other], recv_sem=rs.at[a2a + other],
-            device_id=(sp, other), device_id_type=MESH,
-        )
 
     @scoped("a2a_wait")
     def a2a_wait():
         local["ow"].wait()
         local["st"].wait()
         local["g1"].wait()
-        for i in range(1, 8):
-            a2a_copy(i).wait_recv()
+        arrive("a2a")
 
     a2a_wait()
+    need("u", (3, 0))
+    need("u", (1, 0))
 
     def project(n):
         cols = pl.ds(n * 512, 512)
@@ -306,7 +310,12 @@
 
     def fs_send(name, src, dst, i, dev, n=HALF):
         rows = pl.ds(i * n, n)
-        send((name, i), fs.at[src[0], src[1], rows, :], fs.at[dst[0], dst[1], rows, :], dev)
+        to_partner = name[0] == "c"
+        send(
+            (name, i), fs.at[src[0], src[1], rows, :], fs.at[dst[0], dst[1], rows, :], dev,
+            "c" if to_partner else name, fs.at[0] if to_partner else fs.at[0, 0],
+            name if to_partner else None, fs.at[1, dst[1]] if to_partner else None,
+        )
 
     @scoped("first_norm")
     def first_norm(h):
@@ -346,8 +355,7 @@
 
     @scoped("hidden_a")
     def hidden_a(dx):
-        for h in range(2):
-            arrive((f"c{dx}", h))
+        arrive(f"c{dx}")
         needs("u", ORDER[: KA // BLK])
         for n in range(HID // 256):
             cols = pl.ds(n * 256, 256)
@@ -356,8 +364,7 @@
 
     @scoped("hidden")
     def hidden(dx):
-        for i in range(4 if dx == 2 else 2):
-            arrive((f"c{dx}", i))
+        arrive(f"c{dx}")
         needs("u", ORDER)
         lo = 0 if dx == 2 else KA
         for n in range(HID // 256):
@@ -374,7 +381,7 @@
         needs("d", ORDER[2 * j : 2 * j + 2])
         cols = pl.ds(j * CW, CW)
         psend[j] = dot(act[1].reshape(4 * BLK, HID), dn_all[:, cols]).astype(BF16).reshape(R, BLK, CW)
-        send(("p", j), psend.at[j], prx.at[j], partner)
+        send(("p", j), psend.at[j], prx.at[j], partner, "p", psend)
 
     @scoped("product_b")
     def product_b(j):
@@ -390,31 +397,27 @@
     def pair_sum(j):
         arrive(("p", j))
         s2[j] = pair(j, 2).astype(BF16)
-        send(("mid_l", j), s2.at[j, LO, :], mid_l.at[j], right)
-        send(("mid_r", j), s2.at[j, HI, :], mid_r.at[j], left)
+        send("mid", s2.at[j, LO, :], mid.at[j, LO, :], right, "s2", s2, ("mid", j), mid.at[j])
+        send("mid", s2.at[j, HI, :], mid.at[j, HI, :], left, "s2", s2, ("mid", j), mid.at[j])
         s1[j, HI, :] = pair(j, 1, HI).astype(BF16)
         s3[j, LO, :] = pair(j, 3, LO).astype(BF16)
-        send(("dir_l", j), s1.at[j, HI, :], fin_l.at[j, HI, :], right)
-        send(("dir_r", j), s3.at[j, LO, :], fin_r.at[j, LO, :], left)
+        send("fin", s1.at[j, HI, :], fin.at[j, 0, HI, :], right, "s1", s1, ("fin", j), fin.at[j])
+        send("fin", s3.at[j, LO, :], fin.at[j, 1, LO, :], left, "s3", s3, ("fin", j), fin.at[j])
         macc[:, pl.ds(j * CW, CW)] = pair(j, 0)
 
     @scoped("middle")
     def middle(j):
-        arrive(("mid_l", j))
-        s1[j, LO, :] = (pair(j, 1, LO) + mid_l[j].astype(F32)).astype(BF16)
-        send(("fin_l", j), s1.at[j, LO, :], fin_l.at[j, LO, :], right)
-        arrive(("mid_r", j))
-        s3[j, HI, :] = (pair(j, 3, HI) + mid_r[j].astype(F32)).astype(BF16)
-        send(("fin_r", j), s3.at[j, HI, :], fin_r.at[j, HI, :], left)
+        arrive(("mid", j))
+        s1[j, LO, :] = (pair(j, 1, LO) + mid[j, LO, :].astype(F32)).astype(BF16)
+        s3[j, HI, :] = (pair(j, 3, HI) + mid[j, HI, :].astype(F32)).astype(BF16)
+        send("fin", s1.at[j, LO, :], fin.at[j, 0, LO, :], right, "s1", s1, ("fin", j), fin.at[j])
+        send("fin", s3.at[j, HI, :], fin.at[j, 1, HI, :], left, "s3", s3, ("fin", j), fin.at[j])
 
     @scoped("total_sum")
     def total_sum(j):
-        for name in ("dir_l", "dir_r", "fin_l", "fin_r"):
-            arrive((name, j))
-        macc[:, pl.ds(j * CW, CW)] += fin_l[j].astype(F32) + fin_r[j].astype(F32)
-
-    need("u", (3, 0))
-    need("u", (1, 0))
+        arrive(("fin", j))
+        macc[:, pl.ds(j * CW, CW)] += fin[j, 0].astype(F32) + fin[j, 1].astype(F32)
+
     need("u", (0, 3))
     need("u", (0, 1))
     need("u", (2, 0))
@@ -434,12 +437,12 @@
     hidden_a(1)
     gather_rows("x_2", 0)
     gather_rows("x_2", 2)
-    need("d", (2, 0))
     gather_rows("x_2", 1)
     gather_rows("x_2", 3)
     hidden(0)
     hidden(1)
     hidden(3)
+    need("d", (2, 0))
     hidden(2)
     need("d", (0, 3))
     need("d", (0, 1))
@@ -502,12 +505,12 @@
 
     @scoped("drain")
     def drain():
-        for copy in sent:
-            copy.wait_send()
-        for i in range(1, 8):
-            a2a_copy(i).wait_send()
+        for kind, key in ends:
+            if kind == "s":
+                wait(kind, key)
 
     drain()
+    assert len(send_sems.index) == SENDS and len(recv_sems.index) == ARRIVALS
 
 
 def far(v):
@@ -528,8 +531,7 @@
             pltpu.VMEM((1024, BLK), BF16),
             pltpu.VMEM((1024 + 2 * BLK, BLK), BF16),
             pltpu.VMEM((8, BLK), jnp.int32),
-            pltpu.VMEM((8, BLK), jnp.int32),
-            pltpu.VMEM((8, BLK), jnp.int32),
+            pltpu.VMEM((16, BLK), jnp.int32),
             pltpu.VMEM((24, BLK), F32),
             pltpu.VMEM((BLK, D), BF16),
             pltpu.VMEM((1024, D), BF16),
@@ -547,13 +549,11 @@
             pltpu.VMEM((NCH, BLK, CW), BF16),
             pltpu.VMEM((NCH, BLK, CW), BF16),
             pltpu.VMEM((NCH, BLK, CW), BF16),
-            pltpu.VMEM((NCH, BLK // 2, CW), BF16),
-            pltpu.VMEM((NCH, BLK // 2, CW), BF16),
             pltpu.VMEM((NCH, BLK, CW), BF16),
-            pltpu.VMEM((NCH, BLK, CW), BF16),
+            pltpu.VMEM((NCH, 2, BLK, CW), BF16),
             pltpu.VMEM((BLK, D), F32),
-            pltpu.SemaphoreType.DMA((128,)),
-            pltpu.SemaphoreType.DMA((128,)),
+            pltpu.SemaphoreType.DMA((SENDS,)),
+            pltpu.SemaphoreType.DMA((ARRIVALS,)),
             pltpu.SemaphoreType.DMA((9,)),
         ],
         compiler_params=pltpu.CompilerParams(

time: 69.5 us -> 67.7 us (0.974)
  Pallas kernels: 68.6 us -> 66.4 us
    pallas_call x1, Pallas kernels: 68.6 us -> 66.4 us  [per_device(): pl.pallas_call(kernel, out_shape=jax.ShapeDtypeStruct(stream.shape, BF16)...]
where the time goes in v5:
time: 67.7 us; the launch traced here: 67.2 us
  Pallas kernels  66.4 us (98%)
  local copies, waits for them, and re-layouts  0.8 us (1%)
    pallas_call x1, Pallas kernels, per_device(): pl.pallas_call(kernel, out_shape=jax.ShapeDtypeStruct(stream.shape, BF16)...  66.4 us

profile of v5, /device:TPU:1, one launch (start us, length us, event | category | flops | bytes accessed | tf_op | source)
XLA Modules:
  0.0 67.2 jit_solution(2770561248155475884)
XLA Ops:
  0.0 66.4 %layer.1 = bf16[128,2048]{1,0:T(8,128)(2,1)S(1)} custom-call(bf16[1024,128]{1,0:T(8,128)(2,1)} %q_h.1, bf16[1024,128]{1,0:T(8,128)(2,1)} %bitcast.4, f32[2]{0:T(128)} %sink_s.1, s32[8,128]{1,0:T(8,128)} %bitcast.7, bf16[128,2048]{1,0:T(8,128)(2,1)} %st_h.1, bf16[1024,2048]{1,0:T(8,128)(2,1)} %ow_h.1, f32[1,2048]{1,0:T(1,128)} %bitcast.5, ...), custom_call_target="tpu_custom_call" | custom-call | tf_op jit(solution)/shard_map/layer/pallas_call | solution.py:523
  66.4 0.8 %copy.12 = bf16[128,2048]{1,0:T(8,128)(2,1)} copy(bf16[128,2048]{1,0:T(8,128)(2,1)S(1)} %layer.1) | data formatting | bytes 1048576

commit v6 on v5

--- a/solution.py
+++ b/solution.py
@@ -380,13 +380,16 @@
     def product_a(j):
         needs("d", ORDER[2 * j : 2 * j + 2])
         cols = pl.ds(j * CW, CW)
-        psend[j] = dot(act[1].reshape(4 * BLK, HID), dn_all[:, cols]).astype(BF16).reshape(R, BLK, CW)
+        for two in (pl.ds(0, 2), pl.ds(2, 2)):
+            v = dot(act[1, two].reshape(2 * BLK, HID), dn_all[:, cols])
+            psend[j, two] = v.astype(BF16).reshape(2, BLK, CW)
         send(("p", j), psend.at[j], prx.at[j], partner, "p", psend)
 
     @scoped("product_b")
     def product_b(j):
         cols = pl.ds(j * CW, CW)
-        pown[j] = dot(act[0].reshape(4 * BLK, HID), dn_all[:, cols]).reshape(R, BLK, CW)
+        for two in (pl.ds(0, 2), pl.ds(2, 2)):
+            pown[j, two] = dot(act[0, two].reshape(2 * BLK, HID), dn_all[:, cols]).reshape(2, BLK, CW)
 
     LO, HI = pl.ds(0, HALF), pl.ds(HALF, HALF)
 
@@ -399,11 +402,16 @@
         s2[j] = pair(j, 2).astype(BF16)
         send("mid", s2.at[j, LO, :], mid.at[j, LO, :], right, "s2", s2, ("mid", j), mid.at[j])
         send("mid", s2.at[j, HI, :], mid.at[j, HI, :], left, "s2", s2, ("mid", j), mid.at[j])
+        if j < 6:
+            direct(j)
+        macc[:, pl.ds(j * CW, CW)] = pair(j, 0)
+
+    @scoped("direct")
+    def direct(j):
         s1[j, HI, :] = pair(j, 1, HI).astype(BF16)
         s3[j, LO, :] = pair(j, 3, LO).astype(BF16)
         send("fin", s1.at[j, HI, :], fin.at[j, 0, HI, :], right, "s1", s1, ("fin", j), fin.at[j])
         send("fin", s3.at[j, LO, :], fin.at[j, 1, LO, :], left, "s3", s3, ("fin", j), fin.at[j])
-        macc[:, pl.ds(j * CW, CW)] = pair(j, 0)
 
     @scoped("middle")
     def middle(j):
@@ -442,50 +450,52 @@
     hidden(0)
     hidden(1)
     hidden(3)
+    need("d", (0, 3))
+    need("d", (0, 1))
     need("d", (2, 0))
     hidden(2)
-    need("d", (0, 3))
-    need("d", (0, 1))
     product_a(0)
     product_b(0)
     product_a(1)
     need("d", (3, 3))
+    pair_sum(0)
     product_b(1)
-    pair_sum(0)
     product_a(2)
+    pair_sum(1)
     product_b(2)
-    pair_sum(1)
     need("d", (1, 1))
+    pair_sum(2)
     product_a(3)
-    pair_sum(2)
     middle(0)
     product_b(3)
     middle(1)
+    product_a(4)
     pair_sum(3)
+    product_b(4)
+    middle(2)
+    pair_sum(4)
     need("d", (2, 3))
     need("d", (2, 1))
-    middle(2)
-    product_a(4)
-    total_sum(0)
-    product_b(4)
-    total_sum(1)
     middle(3)
-    pair_sum(4)
     product_a(5)
-    total_sum(2)
     product_b(5)
     product_a(6)
-    total_sum(3)
+    pair_sum(5)
     product_b(6)
-    pair_sum(5)
     middle(4)
     product_a(7)
     pair_sum(6)
     product_b(7)
     pair_sum(7)
     middle(5)
+    direct(6)
+    direct(7)
+    middle(6)
+    total_sum(0)
+    total_sum(1)
+    total_sum(2)
+    total_sum(3)
     total_sum(4)
-    middle(6)
     middle(7)
     total_sum(5)
     total_sum(6)

time: 67.7 us -> 65.8 us (0.972)
  Pallas kernels: 66.4 us -> 64.9 us
    pallas_call x1, Pallas kernels: 66.4 us -> 64.9 us  [per_device(): pl.pallas_call(kernel, out_shape=jax.ShapeDtypeStruct(stream.shape, BF16)...]
where the time goes in v6:
time: 65.8 us; the launch traced here: 65.7 us
  Pallas kernels  64.9 us (99%)
  local copies, waits for them, and re-layouts  0.8 us (1%)
    pallas_call x1, Pallas kernels, per_device(): pl.pallas_call(kernel, out_shape=jax.ShapeDtypeStruct(stream.shape, BF16)...  64.9 us

profile of v6, /device:TPU:1, one launch (start us, length us, event | category | flops | bytes accessed | tf_op | source)
XLA Modules:
  0.0 65.7 jit_solution(14214724088060240900)
XLA Ops:
  0.0 64.9 %layer.1 = bf16[128,2048]{1,0:T(8,128)(2,1)S(1)} custom-call(bf16[1024,128]{1,0:T(8,128)(2,1)} %q_h.1, bf16[1024,128]{1,0:T(8,128)(2,1)} %bitcast.4, f32[2]{0:T(128)} %sink_s.1, s32[8,128]{1,0:T(8,128)} %bitcast.7, bf16[128,2048]{1,0:T(8,128)(2,1)} %st_h.1, bf16[1024,2048]{1,0:T(8,128)(2,1)} %ow_h.1, f32[1,2048]{1,0:T(1,128)} %bitcast.5, ...), custom_call_target="tpu_custom_call" | custom-call | tf_op jit(solution)/shard_map/layer/pallas_call | solution.py:533
  64.9 0.8 %copy.12 = bf16[128,2048]{1,0:T(8,128)(2,1)} copy(bf16[128,2048]{1,0:T(8,128)(2,1)S(1)} %layer.1) | data formatting | bytes 1048576

commit v7 on v6

--- a/solution.py
+++ b/solution.py
@@ -18,7 +18,7 @@
 HID = 1024
 NCH = 8
 CW = D // NCH
-SENDS, ARRIVALS = 13, 65
+SENDS, ARRIVALS = 13, 66
 
 ORDER = [
     (0, 0), (1, 0), (3, 0), (0, 1), (0, 3), (3, 3), (3, 1), (1, 1),
@@ -31,14 +31,9 @@
     (3, 0): [(AP, 0), (BP, None), (BM, None)],
     (1, 0): [(AM, 1), (BP, None), (BM, None)],
     (2, 0): [(BP, None), (BM, None)],
-    (0, 3): [(BP, 0)],
-    (0, 1): [(BM, 1)],
-    (3, 3): [(BP, None)],
-    (1, 1): [(BM, None)],
-    (2, 3): [(BP, 0)],
-    (2, 1): [(BM, 1)],
 }
-TOGETHER = (((3, 1), (1, 3)), ((0, 2), (3, 2), (1, 2), (2, 2)))
+ONWARD |= {(da, 3): [(BP, 0)] for da in range(R)} | {(da, 1): [(BM, 1)] for da in range(R)}
+TOGETHER = (((0, 2), (3, 2), (1, 2), (2, 2)),)
 KA = HID
 
 
@@ -430,8 +425,10 @@
     need("u", (0, 1))
     need("u", (2, 0))
     need("u", (3, 3))
+    need("u", (3, 1))
     gather_rows("x_l", 0)
     gather_rows("x_r", 1)
+    need("u", (1, 3))
     need("u", (1, 1))
     hidden_a(0)
     gather_rows("x_l", 1)
@@ -458,26 +455,28 @@
     product_b(0)
     product_a(1)
     need("d", (3, 3))
+    need("d", (3, 1))
     pair_sum(0)
     product_b(1)
     product_a(2)
     pair_sum(1)
     product_b(2)
+    need("d", (1, 3))
     need("d", (1, 1))
     pair_sum(2)
     product_a(3)
+    product_b(3)
     middle(0)
-    product_b(3)
-    middle(1)
     product_a(4)
     pair_sum(3)
+    middle(1)
     product_b(4)
     middle(2)
     pair_sum(4)
     need("d", (2, 3))
     need("d", (2, 1))
+    product_a(5)
     middle(3)
-    product_a(5)
     product_b(5)
     product_a(6)
     pair_sum(5)

time: 65.8 us -> 64.8 us (0.985)
  Pallas kernels: 64.9 us -> 63.9 us
    pallas_call x1, Pallas kernels: 64.9 us -> 63.9 us  [per_device(): pl.pallas_call(kernel, out_shape=jax.ShapeDtypeStruct(stream.shape, BF16)...]
where the time goes in v7:
time: 64.8 us; the launch traced here: 64.7 us
  Pallas kernels  63.9 us (99%)
  local copies, waits for them, and re-layouts  0.8 us (1%)
    pallas_call x1, Pallas kernels, per_device(): pl.pallas_call(kernel, out_shape=jax.ShapeDtypeStruct(stream.shape, BF16)...  63.9 us

profile of v7, /device:TPU:1, one launch (start us, length us, event | category | flops | bytes accessed | tf_op | source)
XLA Modules:
  0.0 64.7 jit_solution(7414965104388054215)
XLA Ops:
  0.0 63.9 %layer.1 = bf16[128,2048]{1,0:T(8,128)(2,1)S(1)} custom-call(bf16[1024,128]{1,0:T(8,128)(2,1)} %q_h.1, bf16[1024,128]{1,0:T(8,128)(2,1)} %bitcast.4, f32[2]{0:T(128)} %sink_s.1, s32[8,128]{1,0:T(8,128)} %bitcast.7, bf16[128,2048]{1,0:T(8,128)(2,1)} %st_h.1, bf16[1024,2048]{1,0:T(8,128)(2,1)} %ow_h.1, f32[1,2048]{1,0:T(1,128)} %bitcast.5, ...), custom_call_target="tpu_custom_call" | custom-call | tf_op jit(solution)/shard_map/layer/pallas_call | solution.py:532
  63.9 0.8 %copy.12 = bf16[128,2048]{1,0:T(8,128)(2,1)} copy(bf16[128,2048]{1,0:T(8,128)(2,1)S(1)} %layer.1) | data formatting | bytes 1048576

commit v8 on v7

--- a/solution.py
+++ b/solution.py
@@ -378,7 +378,7 @@
         for two in (pl.ds(0, 2), pl.ds(2, 2)):
             v = dot(act[1, two].reshape(2 * BLK, HID), dn_all[:, cols])
             psend[j, two] = v.astype(BF16).reshape(2, BLK, CW)
-        send(("p", j), psend.at[j], prx.at[j], partner, "p", psend)
+            send("p", psend.at[j, two], prx.at[j, two], partner, "p", psend, ("p", j), prx.at[j])
 
     @scoped("product_b")
     def product_b(j):
@@ -447,11 +447,11 @@
     hidden(0)
     hidden(1)
     hidden(3)
+    hidden(2)
     need("d", (0, 3))
     need("d", (0, 1))
+    product_a(0)
     need("d", (2, 0))
-    hidden(2)
-    product_a(0)
     product_b(0)
     product_a(1)
     need("d", (3, 3))

time: 64.8 us -> 64.9 us (level)
  no operation moved by 1% of the time
where the time goes in v8:
time: 64.9 us; the launch traced here: 64.8 us
  Pallas kernels  64 us (99%)
  local copies, waits for them, and re-layouts  0.8 us (1%)
    pallas_call x1, Pallas kernels, per_device(): pl.pallas_call(kernel, out_shape=jax.ShapeDtypeStruct(stream.shape, BF16)...  64 us

profile of v8, /device:TPU:1, one launch (start us, length us, event | category | flops | bytes accessed | tf_op | source)
XLA Modules:
  0.0 64.8 jit_solution(2574079159484996212)
XLA Ops:
  0.0 64.0 %layer.1 = bf16[128,2048]{1,0:T(8,128)(2,1)S(1)} custom-call(bf16[1024,128]{1,0:T(8,128)(2,1)} %q_h.1, bf16[1024,128]{1,0:T(8,128)(2,1)} %bitcast.4, f32[2]{0:T(128)} %sink_s.1, s32[8,128]{1,0:T(8,128)} %bitcast.7, bf16[128,2048]{1,0:T(8,128)(2,1)} %st_h.1, bf16[1024,2048]{1,0:T(8,128)(2,1)} %ow_h.1, f32[1,2048]{1,0:T(1,128)} %bitcast.5, ...), custom_call_target="tpu_custom_call" | custom-call | tf_op jit(solution)/shard_map/layer/pallas_call | solution.py:532
  64.0 0.8 %copy.12 = bf16[128,2048]{1,0:T(8,128)(2,1)} copy(bf16[128,2048]{1,0:T(8,128)(2,1)S(1)} %layer.1) | data formatting | bytes 1048576
